TPU v7x, 128 devices: a whole 4x4x4 slice. The times are simulated.
128 devices in a mesh: fs: 16 (over z, y), tp: 8 (over x, core).
Axes of the slice: x: 4, y: 4, z: 4, core: 2. Of those that a mesh axis runs over, the one named last changes fastest.
Arguments:
- tokens: bfloat16 [16384, 2048], P(('fs', 'tp')), may hold values from -6 to 6
- first_block_norm_scale: float32 [2048], replicated, may hold values from 0.1 to 1.9
- first_block_gate_matrix: bfloat16 [2048, 5504], P('fs', 'tp'), may hold values from -0.125 to 0.125
- first_block_up_matrix: bfloat16 [2048, 5504], P('fs', 'tp'), may hold values from -0.125 to 0.125
- first_block_down_matrix: bfloat16 [5504, 2048], P('tp', 'fs'), may hold values from -0.078125 to 0.078125
- mixer_norm_scale: float32 [2048], replicated, may hold values from 0.1 to 1.9
- recurrent_input_matrix: bfloat16 [2048, 3072], P('fs', 'tp'), may hold values from -0.125 to 0.125
- output_gate_projection: bfloat16 [2048, 3072], P('fs', 'tp'), may hold values from -0.125 to 0.125
- convolution_kernel: float32 [4, 3072], P(None, 'tp'), may hold values from -2 to 2
- decay_gate_blocks: bfloat16 [16, 192, 192], P('tp'), may hold values from -0.4375 to 0.4375
- input_gate_blocks: bfloat16 [16, 192, 192], P('tp'), may hold values from -0.4375 to 0.4375
- channel_decay_weight: float32 [3072], P('tp'), may hold values from 3.5 to 11.5
- position_decay_extra: float32 [16384], P('fs'), may hold values from -0.7 to 0
- mixer_output_matrix: bfloat16 [3072, 2048], P('tp', 'fs'), may hold values from -0.109375 to 0.109375
- second_block_norm_scale: float32 [2048], replicated, may hold values from 0.1 to 1.9
- second_block_gate_matrix: bfloat16 [2048, 5504], P('fs', 'tp'), may hold values from -0.125 to 0.125
- second_block_up_matrix: bfloat16 [2048, 5504], P('fs', 'tp'), may hold values from -0.125 to 0.125
- second_block_down_matrix: bfloat16 [5504, 2048], P('tp', 'fs'), may hold values from -0.078125 to 0.078125
Outputs:
- layer_out: bfloat16 [16384, 2048], P(('fs', 'tp'))
All inputs are finite; a program needn't handle non-finite values.
Results may differ from a plain program's by a relative error of at most 0.019.
Values may be sent and summed in bfloat16 or wider, within the bound.
A program may use at most 128 MiB of HBM per device.

v0:
```python
import jax
import jax.numpy as jnp
from jax import lax
from jax.sharding import PartitionSpec as P

EPS = 1e-06
RECURRENT_WIDTH = 8.0


def in_one_piece(arrays, axis, dim, along):
    both = jnp.concatenate(arrays, axis=along)
    filled, at, gathered = (lax.all_gather(both, axis, axis=dim, tiled=True), 0, [])
    for a in arrays:
        gathered.append(lax.slice_in_dim(filled, at, at + a.shape[along], axis=along))
        at += a.shape[along]
    return tuple(gathered)


def copy_for_each(x, axis):
    copies = jnp.broadcast_to(x, (lax.axis_size(axis), *x.shape))
    return lax.all_to_all(copies, axis, split_axis=0, concat_axis=0, tiled=True)


def laid_out(tiles, dim):
    lengths = list(tiles.shape[1:])
    lengths[dim] *= tiles.shape[0]
    return jnp.moveaxis(tiles, 0, dim).reshape(lengths)


def gathered_copies(x, axis, dim):
    tiles = copy_for_each(x, axis)
    return laid_out(tiles, dim)


def cut_along(x, dim, devices):
    before, after = (x.shape[:dim], x.shape[dim + 1 :])
    return jnp.moveaxis(x.reshape(*before, devices, -1, *after), dim, 0)


def sent_and_summed(x, axis, dim):
    devices = lax.axis_size(axis)
    tiles = lax.all_to_all(cut_along(x, dim, devices), axis, 0, 0, tiled=True)
    return jnp.sum(tiles.astype(jnp.float32), axis=0)


def normed(input_token_rows, norm_scale_vector):
    values = input_token_rows.astype(jnp.float32)
    square = jnp.mean(values * values, axis=-1, keepdims=True)
    return (values * lax.rsqrt(square + EPS) * norm_scale_vector).astype(jnp.bfloat16)


def combine(earlier, later):
    decay_one, drive_one = earlier
    decay_two, drive_two = later
    return (decay_one * decay_two, decay_two * drive_one + drive_two)


def sublayer(
    residual_activations,
    norm_scale_vector,
    first_weight,
    second_weight,
    out_weight,
    middle,
    sequence,
    row_count,
):
    normal = normed(residual_activations, norm_scale_vector)
    full_first, full_second = in_one_piece((first_weight, second_weight), "fs", 0, 1)
    piece = lax.all_gather(normal, "tp", axis=0, tiled=True)
    projected = middle(
        jnp.dot(piece, full_first, preferred_element_type=jnp.float32),
        jnp.dot(piece, full_second, preferred_element_type=jnp.float32),
    )
    if sequence is not None:
        projected = sequence(projected)
    full_out = gathered_copies(out_weight, "fs", 1)
    picked = lax.slice_in_dim(projected, 0, row_count * lax.axis_size("tp"), axis=0)
    return sent_and_summed(
        jnp.dot(picked, full_out, preferred_element_type=jnp.float32).astype(jnp.bfloat16), "tp", 0
    )


def shards(
    tokens,
    first_block_norm_scale,
    first_block_gate_matrix,
    first_block_up_matrix,
    first_block_down_matrix,
    mixer_norm_scale,
    recurrent_input_matrix,
    output_gate_projection,
    convolution_kernel,
    decay_gate_blocks,
    input_gate_blocks,
    channel_decay_weight,
    position_decay_extra,
    mixer_output_matrix,
    second_block_norm_scale,
    second_block_gate_matrix,
    second_block_up_matrix,
    second_block_down_matrix,
):
    row_count = tokens.shape[0]
    residual_activations = tokens

    def feed_middle(gate_pre, up_pre):
        return (jax.nn.silu(gate_pre) * up_pre).astype(jnp.bfloat16)

    def mixer_middle(recur_pre, branch_pre):
        return jnp.concatenate(
            [recur_pre.astype(jnp.bfloat16), branch_pre.astype(jnp.bfloat16)], axis=1
        )

    def recurrent(projected):
        channels = projected.shape[1] // 2
        length = projected.shape[0]
        recur_rows = projected[:, :channels]
        branch_rows = projected[:, channels:]
        taps = convolution_kernel.shape[0]
        summed = lax.conv_general_dilated(
            recur_rows.astype(jnp.float32)[None],
            convolution_kernel[:, None, :],
            window_strides=(1,),
            padding=((taps - 1, 0),),
            dimension_numbers=("NWC", "WIO", "NWC"),
            feature_group_count=channels,
            precision=lax.Precision.HIGHEST,
        )[0]
        conv_out = summed.astype(jnp.bfloat16)
        grouped = conv_out.reshape(length, decay_gate_blocks.shape[0], decay_gate_blocks.shape[1])
        decay_gate_value = jax.nn.sigmoid(
            jnp.einsum(
                "thi,hij->thj", grouped, decay_gate_blocks, preferred_element_type=jnp.float32
            ).reshape(length, channels)
        )
        input_gate = jax.nn.sigmoid(
            jnp.einsum(
                "thi,hij->thj", grouped, input_gate_blocks, preferred_element_type=jnp.float32
            ).reshape(length, channels)
        )
        log_decay_factor = (
            -RECURRENT_WIDTH * decay_gate_value * jax.nn.softplus(-channel_decay_weight)
            + position_decay_extra[:, None]
        )
        decay_rate = jnp.exp(log_decay_factor)
        drive_in = (
            jnp.sqrt(-jnp.expm1(2.0 * log_decay_factor)) * input_gate * conv_out.astype(jnp.float32)
        )
        _, hidden_state = lax.associative_scan(combine, (decay_rate, drive_in), axis=0)
        return (
            jax.nn.gelu(branch_rows.astype(jnp.float32), approximate=True) * hidden_state
        ).astype(jnp.bfloat16)

    first_out = sublayer(
        residual_activations,
        first_block_norm_scale,
        first_block_gate_matrix,
        first_block_up_matrix,
        first_block_down_matrix,
        feed_middle,
        None,
        row_count,
    )
    residual_activations = (residual_activations.astype(jnp.float32) + 0.5 * first_out).astype(
        jnp.bfloat16
    )
    mixer_output_rows = sublayer(
        residual_activations,
        mixer_norm_scale,
        recurrent_input_matrix,
        output_gate_projection,
        mixer_output_matrix,
        mixer_middle,
        recurrent,
        row_count,
    )
    residual_activations = (residual_activations.astype(jnp.float32) + mixer_output_rows).astype(
        jnp.bfloat16
    )
    second_out = sublayer(
        residual_activations,
        second_block_norm_scale,
        second_block_gate_matrix,
        second_block_up_matrix,
        second_block_down_matrix,
        feed_middle,
        None,
        row_count,
    )
    residual_activations = (residual_activations.astype(jnp.float32) + 0.5 * second_out).astype(
        jnp.bfloat16
    )
    return residual_activations


def solution(mesh):
    in_specs = (
        P(("fs", "tp"), None),
        P(),
        P("fs", "tp"),
        P("fs", "tp"),
        P("tp", "fs"),
        P(),
        P("fs", "tp"),
        P("fs", "tp"),
        P(None, "tp"),
        P("tp", None, None),
        P("tp", None, None),
        P("tp"),
        P("fs"),
        P("tp", "fs"),
        P(),
        P("fs", "tp"),
        P("fs", "tp"),
        P("tp", "fs"),
    )
    out_specs = P(("fs", "tp"), None)
    return jax.shard_map(shards, mesh=mesh, in_specs=in_specs, out_specs=out_specs, check_vma=False)
```

profile of v0, /device:TPU:1, one launch (start us, length us, event | category | flops | bytes accessed | tf_op | source)
XLA Modules:
  0.0 540.3 jit_solution(13397318217952377570)
XLA Ops:
  13.7 8.7 %all-to-all-start = ((bf16[16,688,128]{2,1,0:T(8,128)(2,1)}), bf16[16,688,128]{2,1,0:T(8,128)(2,1)S(1)}, u32[]{:S(2)}, u32[]{:S(2)}) async-start(bf16[16,688,128]{2,1,0:T(8,128)(2,1)} %broadcast_in_dim.10), calls=%async_computation | async-start | bytes 5636096 | tf_op jit(solution)/shard_map/all_to_all | solution.py:21
  23.3 22.4 %all-gather.7.cloned.1.call-done = bf16[1024,2048]{1,0:T(8,128)(2,1)} async-done(((bf16[128,2048]{1,0:T(8,128)(2,1)}), bf16[1024,2048]{1,0:T(8,128)(2,1)}) %all-gather.7.cloned.1.call-update) | async-done | bytes 4194320 | tf_op jit(solution)/shard_map/all_gather | solution.py:70
  45.7 65.6 %all-gather.9.cloned.1.call-done = bf16[2048,1376]{0,1:T(8,128)(2,1)} async-done(((bf16[128,1376]{0,1:T(8,128)(2,1)}), bf16[2048,1376]{0,1:T(8,128)(2,1)}) %all-gather.9.cloned.1.call-update) | async-done | bytes 5636112 | tf_op jit(solution)/shard_map/all_gather | solution.py:12
  111.2 7.7 %fusion.10 = f32[1024,688]{0,1:T(8,128)} fusion(bf16[1024,2048]{1,0:T(8,128)(2,1)} %all-gather.7.cloned.1.call-done, bf16[2048,1376]{0,1:T(8,128)(2,1)} %all-gather.9.cloned.1.call-done), kind=kOutput, calls=%fused_computation.16 | convolution fusion | flops 2885681152 | bytes 9830400 | tf_op jit(solution)/shard_map/dot_general | solution.py:72
  118.9 11.0 %convolution_convert_fusion.2 = bf16[1024,2048]{1,0:T(8,128)(2,1)} fusion(f32[1024,688]{0,1:T(8,128)} %fusion.10, bf16[1024,2048]{1,0:T(8,128)(2,1)} %all-gather.7.cloned.1.call-done, bf16[2048,1376]{0,1:T(8,128)(2,1)} %all-gather.9.cloned.1.call-done, bf16[16,688,128]{2,1,0:T(8,128)(2,1)S(1)} %all-to-all-done), kind=kOutput, calls=%fused_computation.5 | convolution fusion | flops 5777686528 | bytes 16842752 | tf_op jit(solution)/shard_map/dot_general | solution.py:80
  130.0 54.9 %all_to_all.30 = bf16[8,128,2048]{2,1,0:T(8,128)(2,1)S(1)} all-to-all(bf16[8,128,2048]{2,1,0:T(8,128)(2,1)} %bitcast.50), channel_id=1, replica_groups=mesh['fs'=16,'tp'=8] {'tp'}, dimensions={0} | all-to-all | bytes 8388608 | tf_op jit(solution)/shard_map/all_to_all | solution.py:42
  189.6 4.7 all-to-all-start.2
  195.4 23.0 %all-gather.11.cloned.1.call-done = bf16[1024,2048]{1,0:T(8,128)(2,1)} async-done(((bf16[128,2048]{1,0:T(8,128)(2,1)}), bf16[1024,2048]{1,0:T(8,128)(2,1)}) %all-gather.11.cloned.1.call-update) | async-done | bytes 4194320 | tf_op jit(solution)/shard_map/all_gather | solution.py:70
  218.4 5.0 fusion.35
  231.1 3.4 fusion.34
  234.6 2.8 slice.256
  237.4 2.8 slice.257
  240.2 2.8 slice.255
  242.9 2.8 slice.259
  245.7 3.2 fusion.89
  248.8 3.0 slice.262
  251.9 3.1 slice.263
  254.9 3.1 slice.261
  258.0 3.1 slice.265
  327.3 3.1 slice.260
  330.4 3.1 slice.325
  334.8 2.8 slice.327
  337.6 2.8 slice.254
  346.6 3.1 pad.80
  351.3 10.3 %convolution_convert_fusion = bf16[1024,2048]{1,0:T(8,128)(2,1)} fusion(bf16[384,2048]{0,1:T(8,128)(2,1)} %bitcast.12, f32[1024,384]{1,0:T(8,128)S(1)} %pad.79, f32[1024,384]{1,0:T(8,128)} %pad.80, bf16[1024,2048]{1,0:T(8,128)(2,1)} %all-gather.11.cloned.1.call-done, bf16[2048,768]{1,0:T(8,128)(2,1)} %all-gather.13.cloned.1.call-done), kind=kOutput, calls=%fused_computation.3 | convolution fusion | flops 3228434432 | bytes 14680064 | tf_op jit(solution)/shard_map/dot_general | solution.py:80
  361.6 52.5 %all_to_all.31 = bf16[8,128,2048]{2,1,0:T(8,128)(2,1)S(1)} all-to-all(bf16[8,128,2048]{2,1,0:T(8,128)(2,1)} %bitcast.49), channel_id=1, replica_groups=mesh['fs'=16,'tp'=8] {'tp'}, dimensions={0} | all-to-all | bytes 8388608 | tf_op jit(solution)/shard_map/all_to_all | solution.py:42
  418.5 6.7 %all-to-all-start.4 = ((bf16[16,688,128]{2,1,0:T(8,128)(2,1)}), bf16[16,688,128]{2,1,0:T(8,128)(2,1)S(1)}, u32[]{:S(2)}, u32[]{:S(2)}) async-start(bf16[16,688,128]{2,1,0:T(8,128)(2,1)} %broadcast_in_dim.27), calls=%async_computation.4 | async-start | bytes 5636096 | tf_op jit(solution)/shard_map/all_to_all | solution.py:21
  425.3 23.6 %all-gather.15.cloned.1.call-done = bf16[1024,2048]{1,0:T(8,128)(2,1)} async-done(((bf16[128,2048]{1,0:T(8,128)(2,1)}), bf16[1024,2048]{1,0:T(8,128)(2,1)}) %all-gather.15.cloned.1.call-update) | async-done | bytes 4194320 | tf_op jit(solution)/shard_map/all_gather | solution.py:70
  448.9 7.7 %fusion.6 = f32[1024,688]{0,1:T(8,128)} fusion(bf16[1024,2048]{1,0:T(8,128)(2,1)} %all-gather.15.cloned.1.call-done, bf16[2048,1376]{0,1:T(8,128)(2,1)} %all-gather.17.cloned.1.call-done), kind=kOutput, calls=%fused_computation.12 | convolution fusion | flops 2885681152 | bytes 9830400 | tf_op jit(solution)/shard_map/dot_general | solution.py:72
  456.6 9.6 %all-to-all-done.4 = bf16[16,688,128]{2,1,0:T(8,128)(2,1)S(1)} async-done(((bf16[16,688,128]{2,1,0:T(8,128)(2,1)}), bf16[16,688,128]{2,1,0:T(8,128)(2,1)S(1)}, u32[]{:S(2)}, u32[]{:S(2)}) %all-to-all-start.4) | async-done | bytes 2818080 | tf_op jit(solution)/shard_map/all_to_all | solution.py:21
  466.2 11.0 %convolution_convert_fusion.1 = bf16[1024,2048]{1,0:T(8,128)(2,1)} fusion(f32[1024,688]{0,1:T(8,128)} %fusion.6, bf16[1024,2048]{1,0:T(8,128)(2,1)} %all-gather.15.cloned.1.call-done, bf16[2048,1376]{0,1:T(8,128)(2,1)} %all-gather.17.cloned.1.call-done, bf16[16,688,128]{2,1,0:T(8,128)(2,1)S(1)} %all-to-all-done.4), kind=kOutput, calls=%fused_computation.4 | convolution fusion | flops 5777686528 | bytes 16842752 | tf_op jit(solution)/shard_map/dot_general | solution.py:80
  477.3 54.5 %all_to_all.32 = bf16[8,128,2048]{2,1,0:T(8,128)(2,1)S(1)} all-to-all(bf16[8,128,2048]{2,1,0:T(8,128)(2,1)} %bitcast.51), channel_id=1, replica_groups=mesh['fs'=16,'tp'=8] {'tp'}, dimensions={0} | all-to-all | bytes 8388608 | tf_op jit(solution)/shard_map/all_to_all | solution.py:42
  (229 shorter events, 101.9 us)
Async XLA Ops:
  6.5 219.9 %copy-start = (bf16[2,192,192]{2,1,0:T(8,128)(2,1)S(1)}, bf16[2,192,192]{2,1,0:T(8,128)(2,1)}, u32[]{:S(2)}) copy-start(bf16[2,192,192]{2,1,0:T(8,128)(2,1)} %param.27) | copy-start | bytes 442372
  6.5 5.2 copy-start.10
  6.5 39.1 %all-gather.7.cloned.1.call-start = ((), (), s32[]{:S(2)}) async-start(), calls=%async_computation.6 | async-start | bytes 4718592 | tf_op jit(solution)/shard_map/all_gather | solution.py:70
  9.9 101.4 %all-gather.9.cloned.1.call-start = ((), (), s32[]{:S(2)}) async-start(), calls=%async_computation.7 | async-start | bytes 5988352 | tf_op jit(solution)/shard_map/all_gather | solution.py:12
  13.7 8.8 %copy-start.15 = (bf16[128,384]{1,0:T(8,128)(2,1)S(1)}, bf16[128,384]{1,0:T(8,128)(2,1)}, u32[]{:S(2)}) copy-start(bf16[128,384]{1,0:T(8,128)(2,1)} %param.25) | copy-start | bytes 294916
  13.7 8.8 %copy-start.16 = (bf16[128,384]{1,0:T(8,128)(2,1)S(1)}, bf16[128,384]{1,0:T(8,128)(2,1)}, u32[]{:S(2)}) copy-start(bf16[128,384]{1,0:T(8,128)(2,1)} %param.24) | copy-start | bytes 294916
  13.7 105.2 %all-to-all-start = ((bf16[16,688,128]{2,1,0:T(8,128)(2,1)}), bf16[16,688,128]{2,1,0:T(8,128)(2,1)S(1)}, u32[]{:S(2)}, u32[]{:S(2)}) async-start(bf16[16,688,128]{2,1,0:T(8,128)(2,1)} %broadcast_in_dim.10), calls=%async_computation | async-start | bytes 5636096 | tf_op jit(solution)/shard_map/all_to_all | solution.py:21
  22.5 172.9 %all-gather.13.cloned.1.call-start = ((), (), s32[]{:S(2)}) async-start(), calls=%async_computation.9 | async-start | bytes 3342336 | tf_op jit(solution)/shard_map/all_gather | solution.py:12
  23.2 195.2 %all-gather.11.cloned.1.call-start = ((), (), s32[]{:S(2)}) async-start(), calls=%async_computation.8 | async-start | bytes 4718592 | tf_op jit(solution)/shard_map/all_gather | solution.py:70
  188.0 6.3 %copy-start.11 = (bf16[128,688]{0,1:T(8,128)(2,1)S(1)}, bf16[128,688]{0,1:T(8,128)(2,1)}, u32[]{:S(2)}) copy-start(bf16[128,688]{0,1:T(8,128)(2,1)} %param.34) | copy-start | bytes 528388
  188.0 6.3 %copy-start.12 = (bf16[128,688]{0,1:T(8,128)(2,1)S(1)}, bf16[128,688]{0,1:T(8,128)(2,1)}, u32[]{:S(2)}) copy-start(bf16[128,688]{0,1:T(8,128)(2,1)} %param.33) | copy-start | bytes 528388
  188.2 7.1 %copy-start.35 = (f32[384]{0:T(512)S(1)}, f32[384]{0:T(512)}, u32[]{:S(2)}) copy-start(f32[384]{0:T(512)} %param.29) | copy-start | bytes 4612
  189.6 161.7 %all-to-all-start.2 = ((bf16[16,384,128]{1,2,0:T(8,128)(2,1)}), bf16[16,384,128]{1,2,0:T(8,128)(2,1)}, u32[]{:S(2)}, u32[]{:S(2)}) async-start(bf16[16,384,128]{1,2,0:T(8,128)(2,1)} %broadcast_in_dim.26), calls=%async_computation.2 | async-start | bytes 3145728 | tf_op jit(solution)/shard_map/all_to_all | solution.py:21
  194.3 231.0 %all-gather.17.cloned.1.call-start = ((), (), s32[]{:S(2)}) async-start(), calls=%async_computation.11 | async-start | bytes 5988352 | tf_op jit(solution)/shard_map/all_gather | solution.py:12
  195.1 253.8 %all-gather.15.cloned.1.call-start = ((), (), s32[]{:S(2)}) async-start(), calls=%async_computation.10 | async-start | bytes 4718592 | tf_op jit(solution)/shard_map/all_gather | solution.py:70
  323.1 17.9 %copy-start.23 = (f32[2,384]{1,0:T(2,128)S(1)}, f32[2,384]{1,0:T(2,128)}, u32[]{:S(2)}) copy-start(f32[2,384]{1,0:T(2,128)} %slice.304) | copy-start | bytes 9220
  323.1 17.9 %copy-start.24 = (f32[2,384]{1,0:T(2,128)S(1)}, f32[2,384]{1,0:T(2,128)}, u32[]{:S(2)}) copy-start(f32[2,384]{1,0:T(2,128)} %slice.305) | copy-start | bytes 9220
  323.1 17.9 %copy-start.27 = (f32[2,384]{1,0:T(2,128)S(1)}, f32[2,384]{1,0:T(2,128)}, u32[]{:S(2)}) copy-start(f32[2,384]{1,0:T(2,128)} %slice.307) | copy-start | bytes 9220
  323.1 18.0 %copy-start.20 = (f32[4,384]{1,0:T(4,128)S(1)}, f32[4,384]{1,0:T(4,128)}, u32[]{:S(2)}) copy-start(f32[4,384]{1,0:T(4,128)} %get-tuple-element.28) | copy-start | bytes 18436
  323.1 18.7 %copy-start.21 = (f32[3,384]{1,0:T(4,128)S(1)}, f32[3,384]{1,0:T(4,128)}, u32[]{:S(2)}) copy-start(f32[3,384]{1,0:T(4,128)} %slice.296) | copy-start | bytes 13828
  323.1 18.7 %copy-start.22 = (f32[3,384]{1,0:T(4,128)S(1)}, f32[3,384]{1,0:T(4,128)}, u32[]{:S(2)}) copy-start(f32[3,384]{1,0:T(4,128)} %slice.313) | copy-start | bytes 13828
  323.1 18.7 %copy-start.32 = (f32[1,384]{1,0:T(1,128)S(1)}, f32[1,384]{1,0:T(1,128)}, u32[]{:S(2)}) copy-start(f32[1,384]{1,0:T(1,128)} %slice.345) | copy-start | bytes 4612
  323.1 18.8 %copy-start.19 = (f32[7,384]{1,0:T(8,128)S(1)}, f32[7,384]{1,0:T(8,128)}, u32[]{:S(2)}) copy-start(f32[7,384]{1,0:T(8,128)} %slice.315) | copy-start | bytes 32260
  323.2 18.8 %copy-start.31 = (f32[1,384]{1,0:T(1,128)S(1)}, f32[1,384]{1,0:T(1,128)}, u32[]{:S(2)}) copy-start(f32[1,384]{1,0:T(1,128)} %slice.344) | copy-start | bytes 4612
  324.3 17.7 %copy-start.17 = (f32[15,384]{1,0:T(8,128)S(1)}, f32[15,384]{1,0:T(8,128)}, u32[]{:S(2)}) copy-start(f32[15,384]{1,0:T(8,128)} %slice.284) | copy-start | bytes 69124
  324.3 17.7 %copy-start.18 = (f32[15,384]{1,0:T(8,128)S(1)}, f32[15,384]{1,0:T(8,128)}, u32[]{:S(2)}) copy-start(f32[15,384]{1,0:T(8,128)} %slice.317) | copy-start | bytes 69124
  324.3 17.8 %copy-start.30 = (f32[1,384]{1,0:T(1,128)S(1)}, f32[1,384]{1,0:T(1,128)}, u32[]{:S(2)}) copy-start(f32[1,384]{1,0:T(1,128)} %slice.343) | copy-start | bytes 4612
  340.4 5.2 copy-start.9
  340.4 5.3 copy-start.29
  346.6 4.4 copy-start.28
  418.5 47.7 %all-to-all-start.4 = ((bf16[16,688,128]{2,1,0:T(8,128)(2,1)}), bf16[16,688,128]{2,1,0:T(8,128)(2,1)S(1)}, u32[]{:S(2)}, u32[]{:S(2)}) async-start(bf16[16,688,128]{2,1,0:T(8,128)(2,1)} %broadcast_in_dim.27), calls=%async_computation.4 | async-start | bytes 5636096 | tf_op jit(solution)/shard_map/all_to_all | solution.py:21
  477.3 56.2 %copy-start.1 = (bf16[2,192,192]{2,1,0:T(8,128)(2,1)S(1)}, bf16[2,192,192]{2,1,0:T(8,128)(2,1)}, u32[]{:S(2)}) copy-start(bf16[2,192,192]{2,1,0:T(8,128)(2,1)} %param.27) | copy-start | bytes 442372
  (16 other events, 23.8 us)
Sparse Core Ops, SparseCore 0:
  10.0 35.6 all-gather.6
  47.8 63.4 all-gather.8
  113.4 47.9 all-gather.12
  188.2 30.1 all-gather.10
  220.4 62.0 all-gather.16
  416.6 32.2 all-gather.14
where the time goes:
time: 544 us; the launch traced here: 540 us
  blocking collectives  162 us (30%)
  waiting for transfers between devices  144 us (26%)
  local copies, waits for them, and re-layouts  108 us (20%)
  matrix products  55.6 us (10%)
  other arithmetic  35.3 us (6%)
  starting transfers between devices  20.5 us (4%)
  between operations  14.4 us (3%)
    all_to_all x3, blocking collectives, sent_and_summed(): tiles = lax.all_to_all(cut_along(x, dim, devices), axis, 0, 0, tiled=True)  162 us
    slice x60, local copies, waits for them, and re-layouts, recurrent(): lax.associative_scan(combine, (decay_rate, drive_in), axis=0)  92.2 us
    all_gather x3, waiting for transfers between devices, sublayer(): piece = lax.all_gather(normal, 'tp', axis=0, tiled=True)  69 us
    all_gather x3, waiting for transfers between devices, in_one_piece(): lax.all_gather(both, axis, axis=dim, tiled=True)  65.6 us
    dot_general x3, matrix products, sublayer(): jnp.dot(picked, full_out, preferred_element_type=jnp.float32)  32.4 us
    dot_general x3, matrix products, sublayer(): jnp.dot(piece, full_first, preferred_element_type=jnp.float32)  20.4 us
    all_to_all x3, starting transfers between devices, copy_for_each(): return lax.all_to_all(copies, axis, split_axis=0, concat_axis=0, tiled=True)  20.1 us
    mul x8, other arithmetic, combine(): return (decay_one * decay_two, decay_two * drive_one + drive_two)  14.1 us
  transfers between devices with their start and end apart: 9, of which 5 were waited for; matrix products, arithmetic and copies ran while one was open for 34% of the time, Pallas kernels for 0%

commit v1 on v0

v1 whole, which is shorter than its diff:
```python
import functools

import jax
import jax.numpy as jnp
from jax import lax
from jax.experimental import pallas as pl
from jax.experimental.pallas import tpu as pltpu
from jax.sharding import PartitionSpec as P

EPS = 1e-06
MESH = pl.DeviceIdType.MESH
F32 = jnp.float32
BF16 = jnp.bfloat16

ROWS = 128
HALF = ROWS // 2
D = 2048
NFS = 16
HID = 688
HPAD = 768
CH = 384
SEQ = 1024
FULL_TILES = HID // 128
FFN_ROWS = HID + 2 * FULL_TILES * 128 + 128
MIX_ROWS = 3 * CH
FFN_CUTS = (0, 528, 1056, 1584, 2096)
MIX_CUTS = (0, 288, 576, 864, 1152)


def sigmoid(v):
    return 1.0 / (1.0 + jnp.exp(-v))


def one_minus_exp(v):
    series = 1.0 / 720.0 + v * (1.0 / 5040.0)
    for term in (1.0 / 120.0, 1.0 / 24.0, 1.0 / 6.0, 0.5, 1.0):
        series = term + v * series
    return jnp.where(v > -0.3, -v * series, 1.0 - jnp.exp(v))


def layer_kernel(
    tok, s1, s2, s3,
    g1, u1, t1, d1, ri, og, mo, g3, u3, t3, d3,
    ck, gb, cv, pde,
    out,
    w1, w2, w3, xg, hid, ps, pr, po, sb, rb, res, rc, br, sa, sd,
    wl, ws, wr, ags, agr, prs, prr, rss, rsr,
):
    fs = lax.axis_index("fs")
    tp = lax.axis_index("tp")
    z, y = fs // 4, fs % 4
    x, c = tp // 2, tp % 2

    def chip(dx):
        return (x + dx) % 4

    def dev_x(dx):
        return (fs, chip(dx) * 2 + c)

    partner = (fs, x * 2 + (1 - c))
    right, left = dev_x(1), dev_x(3)

    def fs_of(dz, dy):
        return ((z + dz) % 4) * 4 + (y + dy) % 4

    def rcopy(src, dst, ssem, rsem, dev):
        return pltpu.make_async_remote_copy(
            src_ref=src, dst_ref=dst, send_sem=ssem, recv_sem=rsem,
            device_id=dev, device_id_type=MESH,
        )

    def load_ffn(w, g, u, t, d, sem):
        pltpu.make_async_copy(d, w.at[fs, pl.ds(0, HID)], sem).start()
        for j in range(FULL_TILES):
            cols = pl.ds(j * 128, 128)
            pltpu.make_async_copy(g.at[:, cols], w.at[fs, pl.ds(HID + j * 128, 128)], sem).start()
            pltpu.make_async_copy(
                u.at[:, cols], w.at[fs, pl.ds(HID + (FULL_TILES + j) * 128, 128)], sem
            ).start()
        pltpu.make_async_copy(t, w.at[fs, pl.ds(HID + 2 * FULL_TILES * 128, 128)], sem).start()

    def load_mix(w, sem):
        pltpu.make_async_copy(mo, w.at[fs, pl.ds(0, CH)], sem).start()
        for j in range(CH // 128):
            cols = pl.ds(j * 128, 128)
            pltpu.make_async_copy(ri.at[:, cols], w.at[fs, pl.ds(CH + j * 128, 128)], sem).start()
            pltpu.make_async_copy(og.at[:, cols], w.at[fs, pl.ds(2 * CH + j * 128, 128)], sem).start()

    def wait_load(w, sem):
        pltpu.make_async_copy(w.at[fs], w.at[fs], sem).wait()

    def weight_steps(n, w, cuts):
        def block(h, dp, dq):
            return fs_of(dq, dp) if h == 0 else fs_of(dp, dq)

        def rows(h, part):
            lo, mid, hi = cuts[2 * h], cuts[2 * h + 1], cuts[2 * h + 2]
            a, b = {"all": (lo, hi), "first": (lo, mid), "second": (mid, hi)}[part]
            return pl.ds(a, b - a)

        started = []

        def desc(h, dp, dq, part, k, to):
            ref = w.at[block(h, dp, dq), rows(h, part)]
            return rcopy(ref, ref, ws.at[n, 20 * h + k], wr.at[n, 20 * h + k], (block(h, *to), tp))

        def send(*a):
            cp = desc(*a)
            cp.start()
            started.append(cp)

        def recv(h, dp, dq, part, k):
            desc(h, dp, dq, part, k, (0, 0)).wait_recv()

        offs = (0, 3, 1, 2)

        def start():
            for h in (0, 1):
                send(h, 0, 0, "all", 0, (1, 0))
                send(h, 0, 0, "all", 1, (3, 0))
            for h in (0, 1):
                send(h, 0, 0, "all", 4, (0, 1))
                send(h, 0, 0, "all", 5, (0, 3))

        def across(h, j):
            send(h, offs[j], 0, "all", 4 + 4 * j, (0, 1))
            send(h, offs[j], 0, "all", 5 + 4 * j, (0, 3))

        def near(j):
            for h in (0, 1):
                recv(h, offs[j], 0, "all", j - 1)
                if j == 1:
                    send(h, 3, 0, "first", 2, (1, 0))
                else:
                    send(h, 1, 0, "second", 3, (3, 0))
            for h in (0, 1):
                across(h, j)

        def far():
            for h in (0, 1):
                recv(h, 2, 0, "first", 2)
                recv(h, 2, 0, "second", 3)
                across(h, 3)

        def forward(j):
            for h in (0, 1):
                recv(h, offs[j], 3, "all", 4 + 4 * j)
                send(h, offs[j], 3, "first", 6 + 4 * j, (0, 1))
            for h in (0, 1):
                recv(h, offs[j], 1, "all", 5 + 4 * j)
                send(h, offs[j], 1, "second", 7 + 4 * j, (0, 3))

        def last():
            for j in range(4):
                for h in (0, 1):
                    recv(h, offs[j], 2, "first", 6 + 4 * j)
                    recv(h, offs[j], 2, "second", 7 + 4 * j)

        def drain():
            for cp in started:
                cp.wait_send()

        return [
            start,
            functools.partial(near, 1),
            functools.partial(near, 2),
            functools.partial(forward, 0),
            far,
            functools.partial(forward, 1),
            functools.partial(forward, 2),
            functools.partial(forward, 3),
            last,
            drain,
        ]

    def gather_steps(l):
        lo, hi = pl.ds(0, HALF), pl.ds(HALF, HALF)
        started = []

        def blk(dx, same=True):
            return chip(dx) * 2 + (c if same else 1 - c)

        def send(ref, k, dev):
            cp = rcopy(ref, ref, ags.at[l, k], agr.at[l, k], dev)
            cp.start()
            started.append(cp)

        def recv(ref, k):
            rcopy(ref, ref, ags.at[l, k], agr.at[l, k], partner).wait_recv()

        def start():
            mine = xg.at[blk(0)]
            send(xg.at[blk(0), lo], 1, right)
            send(xg.at[blk(0), hi], 2, left)
            send(xg.at[blk(0), hi], 3, right)
            send(xg.at[blk(0), lo], 4, left)
            send(mine, 0, partner)

        def forward():
            recv(xg.at[blk(3), lo], 1)
            send(xg.at[blk(3), lo], 5, right)
            recv(xg.at[blk(1), hi], 2)
            send(xg.at[blk(1), hi], 6, left)

        def near():
            recv(xg.at[blk(3), hi], 3)
            send(xg.at[blk(3)], 7, partner)
            recv(xg.at[blk(1), lo], 4)
            send(xg.at[blk(1)], 8, partner)

        def far():
            recv(xg.at[blk(2), lo], 5)
            recv(xg.at[blk(2), hi], 6)
            send(xg.at[blk(2)], 9, partner)

        def ready(dx):
            recv(xg.at[blk(dx, False)], {0: 0, 3: 7, 1: 8, 2: 9}[dx])

        def drain():
            for cp in started:
                cp.wait_send()

        return start, forward, near, far, ready, drain

    def normed(values, scale):
        square = jnp.mean(values * values, axis=-1, keepdims=True)
        return (values * lax.rsqrt(square + EPS) * scale[...]).astype(BF16)

    G = 16

    def first_norm():
        def body(i, _):
            r = pl.ds(pl.multiple_of(i * G, G), G)
            xg[tp, r, :] = normed(tok[r, :].astype(F32), s1)
            return 0

        lax.fori_loop(0, ROWS // G, body, 0)

    def ffn_in(w, dx):
        xd = chip(dx)
        lhs = xg[pl.ds(2 * xd, 2)].reshape(2 * ROWS, D)

        def tile(at):
            return w[:, pl.ds(pl.multiple_of(at, 16), 128), :].reshape(D, 128)

        def body(j, _):
            rhs = jnp.concatenate([tile(HID + j * 128), tile(HID + (FULL_TILES + j) * 128)], axis=1)
            r = jnp.dot(lhs, rhs, preferred_element_type=F32)
            g, u = r[:, :128], r[:, 128:]
            h = (g * sigmoid(g) * u).astype(BF16)
            hid[pl.ds(2 * xd, 2), :, pl.ds(pl.multiple_of(j * 128, 128), 128)] = h.reshape(2, ROWS, 128)
            return 0

        lax.fori_loop(0, FULL_TILES, body, 0)
        r = jnp.dot(lhs, tile(HID + 2 * FULL_TILES * 128), preferred_element_type=F32)
        u = pltpu.roll(r, 128 - (HID - FULL_TILES * 128), 1)
        lane = lax.broadcasted_iota(jnp.int32, r.shape, 1)
        h = jnp.where(lane < HID - FULL_TILES * 128, r * sigmoid(r) * u, 0.0).astype(BF16)
        hid[pl.ds(2 * xd, 2), :, pl.ds(FULL_TILES * 128, 128)] = h.reshape(2, ROWS, 128)

    def mix_in(dx):
        xd = chip(dx)
        lhs = xg[pl.ds(2 * xd, 2)].reshape(2 * ROWS, D)

        def tile(at):
            return w2[:, pl.ds(pl.multiple_of(at, 16), 128), :].reshape(D, 128)

        def body(j, _):
            rhs = jnp.concatenate([tile(CH + j * 128), tile(2 * CH + j * 128)], axis=1)
            r = jnp.dot(lhs, rhs, preferred_element_type=F32).astype(BF16)
            cols = pl.ds(pl.multiple_of(j * 128, 128), 128)
            rc[pl.ds(pl.multiple_of(8 + xd * 256, 8), 256), cols] = r[:, :128].astype(F32)
            br[pl.ds(pl.multiple_of(xd * 256, 256), 256), cols] = r[:, 128:]
            return 0

        lax.fori_loop(0, CH // 128, body, 0)

    def gates(i):
        at = pl.multiple_of(i * 256, 256)
        tiles = []
        for j in range(CH // 128):
            cols = pl.ds(j * 128, 128)
            window = rc[pl.ds(at, 264), cols]
            acc = window[8:] * ck[3:4, cols]
            for s in (1, 2, 3):
                acc = acc + pltpu.roll(window, s, 0)[8:] * ck[3 - s : 4 - s, cols]
            tiles.append(acc.astype(BF16))
        conv = jnp.concatenate(tiles, axis=1)
        both = jnp.dot(conv, gb[...], preferred_element_type=F32)
        extra = pde[pl.ds(at, 256), :]
        for j in range(CH // 128):
            cols = pl.ds(j * 128, 128)
            rate = sigmoid(both[:, j * 128 : (j + 1) * 128])
            gate = sigmoid(both[:, CH + j * 128 : CH + (j + 1) * 128])
            log_a = rate * cv[:, cols] + extra
            sa[pl.ds(at, 256), cols] = jnp.exp(log_a)
            sd[pl.ds(at, 256), cols] = (
                jnp.sqrt(one_minus_exp(2.0 * log_a)) * gate * tiles[j].astype(F32)
            )

    T = 64

    def scan_chunk(i, carry):
        r = pl.ds(pl.multiple_of(i * T, T), T)
        a, b = sa[r, :], sd[r, :]
        row = lax.broadcasted_iota(jnp.int32, (T, CH), 0)
        s = 1
        while s < T:
            here = row >= s
            b = a * jnp.where(here, pltpu.roll(b, s, 0), 0.0) + b
            a = a * jnp.where(here, pltpu.roll(a, s, 0), 1.0)
            s *= 2
        state = b + a * carry
        v = br[r, :].astype(F32)
        gelu = 0.5 * v * (1.0 + jnp.tanh(0.7978845608028654 * (v + 0.044715 * v * v * v)))
        hid[i // 2, pl.ds(pl.multiple_of((i % 2) * T, T), T), pl.ds(0, CH)] = (gelu * state).astype(BF16)
        return state[T - 1 : T, :]

    SLOT = {2: 0, 1: 1, 3: 2, 0: 3}

    def project(l, w, depth, dx):
        xd = chip(dx)
        k = SLOT[dx]
        lhs = jnp.concatenate(
            [hid[2 * xd + 1 - c, :, pl.ds(0, depth)], hid[2 * xd + c, :, pl.ds(0, depth)]], axis=0
        )

        def body(n, _):
            rhs = jnp.concatenate([w[2 * n, pl.ds(0, depth), :], w[2 * n + 1, pl.ds(0, depth), :]], axis=1)
            r = jnp.dot(lhs, rhs, preferred_element_type=F32).astype(BF16)
            cols = pl.ds(pl.multiple_of(n * 256, 256), 256)
            ps[k, :, cols] = r[:ROWS]
            po[k, :, cols] = r[ROWS:]
            return 0

        lax.fori_loop(0, NFS // 2, body, 0)
        rcopy(ps.at[k], pr.at[k], prs.at[l, k], prr.at[l, k], partner).start()

    def pair_ready(l, dx):
        k = SLOT[dx]
        rcopy(ps.at[k], pr.at[k], prs.at[l, k], prr.at[l, k], partner).wait_recv()

    def pair(k, r):
        return po[k, r, :].astype(F32) + pr[k, r, :].astype(F32)

    def ring(l, way, slot):
        return rcopy(
            sb.at[way, slot], rb.at[way, slot], rss.at[l, way, slot], rsr.at[l, way, slot],
            (right, left)[way],
        )

    def post(l, way, slot, dx, base, extra=None):
        def body(i, _):
            at = pl.multiple_of(i * G, G)
            v = pair(SLOT[dx], pl.ds(base + at, G))
            if extra is not None:
                v = v + rb[way, extra, pl.ds(at, G), :].astype(F32)
            sb[way, slot, pl.ds(at, G), :] = v.astype(BF16)
            return 0

        lax.fori_loop(0, HALF // G, body, 0)
        ring(l, way, slot).start()

    def finish(l, before, weight, scale, result):
        ring(l, 0, 2).wait_recv()
        ring(l, 1, 1).wait_recv()
        for base, a, b in ((0, 2, 1), (HALF, 1, 2)):
            if base:
                ring(l, 0, 1).wait_recv()
                ring(l, 1, 2).wait_recv()

            def body(i, _):
                at = pl.multiple_of(i * G, G)
                r = pl.ds(base + at, G)
                v = pair(SLOT[0], r)
                v = v + rb[0, a, pl.ds(at, G), :].astype(F32) + rb[1, b, pl.ds(at, G), :].astype(F32)
                v = (before[r, :].astype(F32) + weight * v).astype(BF16)
                result[r, :] = v
                if scale is not None:
                    xg[tp, r, :] = normed(v.astype(F32), scale)
                return 0

            lax.fori_loop(0, HALF // G, body, 0)

    def reduce(l, w, depth, before, weight, scale, result, steps):
        steps = iter(steps)

        def step():
            for s in next(steps, ()):
                s()

        project(l, w, depth, 2)
        step()
        project(l, w, depth, 1)
        pair_ready(l, 2)
        post(l, 0, 0, 2, 0)
        post(l, 1, 0, 2, HALF)
        step()
        project(l, w, depth, 3)
        pair_ready(l, 1)
        post(l, 0, 1, 1, HALF)
        project(l, w, depth, 0)
        pair_ready(l, 3)
        post(l, 1, 1, 3, 0)
        step()
        ring(l, 0, 0).wait_recv()
        post(l, 0, 2, 1, 0, extra=0)
        ring(l, 1, 0).wait_recv()
        post(l, 1, 2, 3, HALF, extra=0)
        step()
        pair_ready(l, 0)
        finish(l, before, weight, scale, result)
        for k in range(4):
            rcopy(ps.at[k], pr.at[k], prs.at[l, k], prr.at[l, k], partner).wait_send()
        for way in (0, 1):
            for slot in range(3):
                ring(l, way, slot).wait_send()

    load_ffn(w1, g1, u1, t1, d1, wl.at[0])
    load_mix(w2, wl.at[1])
    load_ffn(w3, g3, u3, t3, d3, wl.at[2])

    barrier = pltpu.get_barrier_semaphore()
    peers = [right, left, partner] + [(fs_of(*d), tp) for d in ((0, 1), (0, 3), (1, 0), (3, 0))]
    for dev in peers:
        pl.semaphore_signal(barrier, inc=1, device_id=dev, device_id_type=MESH)
    first_norm()
    rc[pl.ds(0, 8), :] = jnp.zeros((8, CH), F32)
    pl.semaphore_wait(barrier, len(peers))

    a1 = weight_steps(0, w1, FFN_CUTS)
    a2 = weight_steps(1, w2, MIX_CUTS)
    a3 = weight_steps(2, w3, FFN_CUTS)

    wait_load(w1, wl.at[0])
    a1[0]()
    start, forward, near, far, ready, drain = gather_steps(0)
    start()
    a1[1]()
    a1[2]()
    forward()
    a1[3]()
    near()
    a1[4]()
    far()
    a1[5]()
    for dx in (0, 3, 1, 2):
        ready(dx)
    drain()
    wait_load(w2, wl.at[1])
    wait_load(w3, wl.at[2])
    a1[6]()
    a1[7]()
    a2[0]()
    a1[8]()
    for i, dx in enumerate((2, 1, 3, 0)):
        ffn_in(w1, dx)
        if i == 1:
            a2[1]()
        if i == 2:
            a2[2]()
        if i == 3:
            a2[3]()
    reduce(0, w1, HPAD, tok, 0.5, s2, res, [[a2[4]], [a2[5]], [a2[6]], [a2[7], a3[0]]])

    start, forward, near, far, ready, drain = gather_steps(1)
    start()
    a2[8]()
    ready(0)
    mix_in(0)
    forward()
    a3[1]()
    near()
    a3[2]()
    ready(3)
    mix_in(3)
    ready(1)
    mix_in(1)
    far()
    a3[3]()
    ready(2)
    mix_in(2)
    drain()
    a3[4]()

    def gate_body(i, _):
        gates(i)
        return 0

    lax.fori_loop(0, SEQ // 256, gate_body, 0)
    a3[5]()
    lax.fori_loop(0, SEQ // T, scan_chunk, jnp.zeros((1, CH), F32))
    reduce(1, w2, CH, res, 1.0, s3, res, [[a3[6]], [], [a3[7]], []])

    start, forward, near, far, ready, drain = gather_steps(2)
    start()
    a3[8]()
    ready(0)
    ffn_in(w3, 0)
    forward()
    near()
    ready(3)
    ffn_in(w3, 3)
    ready(1)
    ffn_in(w3, 1)
    far()
    ready(2)
    ffn_in(w3, 2)
    drain()
    reduce(2, w3, HPAD, res, 0.5, None, out, [])
    a1[9]()
    a2[9]()
    a3[9]()


def gate_map(decay, inputs):
    def diagonal(b):
        return jnp.concatenate(
            [jnp.pad(b[0], ((0, 0), (0, 192))), jnp.pad(b[1], ((0, 0), (192, 0)))], axis=0
        )

    return jnp.concatenate([diagonal(decay), diagonal(inputs)], axis=1)


def tail(gate, up):
    at = FULL_TILES * 128
    left = gate.shape[1] - at
    return jnp.concatenate(
        [gate[:, at:], up[:, at:], jnp.zeros((gate.shape[0], 128 - 2 * left), gate.dtype)], axis=1
    )


def shards(
    tokens, s1, g1, u1, d1, s2, ri, og, ck, decay, inputs, cdw, extra, mo, s3, g3, u3, d3
):
    vmem = pl.BlockSpec(memory_space=pltpu.VMEM)
    hbm = pl.BlockSpec(memory_space=pl.ANY)
    row = lambda v: v.reshape(1, -1)
    dma = pltpu.SemaphoreType.DMA
    return pl.pallas_call(
        layer_kernel,
        out_shape=jax.ShapeDtypeStruct((ROWS, D), BF16),
        in_specs=[vmem] * 4 + [hbm] * 11 + [vmem] * 4,
        out_specs=vmem,
        scratch_shapes=[
            pltpu.VMEM((NFS, FFN_ROWS, 128), BF16),
            pltpu.VMEM((NFS, MIX_ROWS, 128), BF16),
            pltpu.VMEM((NFS, FFN_ROWS, 128), BF16),
            pltpu.VMEM((8, ROWS, D), BF16),
            pltpu.VMEM((8, ROWS, HPAD), BF16),
            pltpu.VMEM((4, ROWS, D), BF16),
            pltpu.VMEM((4, ROWS, D), BF16),
            pltpu.VMEM((4, ROWS, D), BF16),
            pltpu.VMEM((2, 3, HALF, D), BF16),
            pltpu.VMEM((2, 3, HALF, D), BF16),
            pltpu.VMEM((ROWS, D), BF16),
            pltpu.VMEM((SEQ + 8, CH), F32),
            pltpu.VMEM((SEQ, CH), BF16),
            pltpu.VMEM((SEQ, CH), F32),
            pltpu.VMEM((SEQ, CH), F32),
            dma((3,)),
            dma((3, 40)),
            dma((3, 40)),
            dma((3, 10)),
            dma((3, 10)),
            dma((3, 4)),
            dma((3, 4)),
            dma((3, 2, 3)),
            dma((3, 2, 3)),
        ],
        compiler_params=pltpu.CompilerParams(
            collective_id=0, has_side_effects=True, vmem_limit_bytes=60 * 1024 * 1024
        ),
        name="layer",
    )(
        tokens, row(s1), row(s2), row(s3),
        g1, u1, tail(g1, u1), d1, ri, og, mo, g3, u3, tail(g3, u3), d3,
        ck, gate_map(decay, inputs), row(-8.0 * jax.nn.softplus(-cdw)),
        jnp.broadcast_to(extra[:, None], (SEQ, 128)),
    )


def solution(mesh):
    in_specs = (
        P(("fs", "tp"), None), P(), P("fs", "tp"), P("fs", "tp"), P("tp", "fs"),
        P(), P("fs", "tp"), P("fs", "tp"), P(None, "tp"), P("tp", None, None),
        P("tp", None, None), P("tp"), P("fs"), P("tp", "fs"), P(),
        P("fs", "tp"), P("fs", "tp"), P("tp", "fs"),
    )
    out_specs = P(("fs", "tp"), None)
    return jax.shard_map(shards, mesh=mesh, in_specs=in_specs, out_specs=out_specs, check_vma=False)
```

time: 544 us -> 206 us (0.38)
  Pallas kernels: 0 us -> 197 us
  blocking collectives: 162 us -> 0 us
  waiting for transfers between devices: 144 us -> 0 us
  local copies, waits for them, and re-layouts: 108 us -> 6.11 us
  matrix products: 55.6 us -> 0 us
  other arithmetic: 35.3 us -> 2.35 us
  starting transfers between devices: 20.5 us -> 0 us
  between operations: 14.4 us -> 0.16 us
    pallas_call x0 -> x1, Pallas kernels: none -> 197 us  [shards(): pl.pallas_call(layer_kernel, out_shape=jax.ShapeDtypeStruct((ROWS, D), BF...]
    all_to_all x3 -> x0, blocking collectives: 162 us -> none  [sent_and_summed(): tiles = lax.all_to_all(cut_along(x, dim, devices), axis, 0, 0, tiled=True)]
    all_gather x6 -> x0, waiting for transfers between devices: 135 us -> none  [the longest x3 69 us: sublayer(): piece = lax.all_gather(normal, 'tp', axis=0, tiled=True)]
    slice x60 -> x4, local copies, waits for them, and re-layouts: 92.2 us -> 0.02 us  [the longest x2 0.01 us: tail(): gate[:, at:]]
    dot_general x8 -> x0, matrix products: 54.1 us -> none  [the longest x3 32.4 us: sublayer(): jnp.dot(picked, full_out, preferred_element_type=jnp.float32)]
    all_to_all x3 -> x0, starting transfers between devices: 20.1 us -> none  [copy_for_each(): return lax.all_to_all(copies, axis, split_axis=0, concat_axis=0, tiled=True)]
    mul x9 -> x1, other arithmetic: 14.1 us -> 0.69 us  [shards(): -8.0 * jax.nn.softplus(-cdw)]
    all_to_all x3 -> x0, waiting for transfers between devices: 9.65 us -> none  [copy_for_each(): return lax.all_to_all(copies, axis, split_axis=0, concat_axis=0, tiled=True)]
  transfers between devices with their start and end apart: 9 -> 0, of which waited for: 5 -> 0; matrix products, arithmetic and copies ran while one was open for 34% -> 0% of each run, Pallas kernels for 0% -> 0%
where the time goes in v1:
time: 206 us
  Pallas kernels  197 us (96%)
  local copies, waits for them, and re-layouts  6.11 us (3%)
  other arithmetic  2.35 us (1%)
    pallas_call x1, Pallas kernels, shards(): pl.pallas_call(layer_kernel, out_shape=jax.ShapeDtypeStruct((ROWS, D), BF...  197 us
    unnamed x23, local copies, waits for them, and re-layouts  4.46 us

profile of v1, /device:TPU:1, one launch (start us, length us, event | category | flops | bytes accessed | tf_op | source)
XLA Modules:
  0.0 205.5 jit_solution(1437674062120194056)
XLA Ops:
  0.0 0.0 copy-start.6
  0.0 0.1 pad.27.clone
  0.1 0.7 fusion.15
  0.8 0.5 reshape.16.cv
  1.3 0.0 copy-start.7
  1.3 1.1 copy.23.g1
  2.4 0.0 copy-start
  2.4 1.1 copy.24.u1
  3.6 0.0 copy-start.1
  3.6 0.0 copy-start.4
  3.6 0.0 copy-start.5
  3.6 0.0 copy-done.6
  3.6 0.1 copy.25.g3
  3.8 0.0 copy-start.2
  3.8 0.0 copy-done.7
  3.8 0.1 copy.26.u3
  4.0 0.0 copy-done
  4.0 0.0 copy-start.3
  4.0 0.7 maximum_maximum_fusion.1
  4.7 0.0 copy-done.4
  4.7 0.0 copy-done.5
  4.8 0.0 copy-done.1
  4.8 0.0 copy-done.2
  4.8 0.0 copy-start.8
  4.8 0.9 fusion.13.gb
  5.7 0.0 copy-done.3
  5.7 0.0 copy-done.8
  5.7 1.0 broadcast_in_dim.2.pde
  6.7 196.9 %layer.1 = bf16[128,2048]{1,0:T(8,128)(2,1)} custom-call(bf16[128,2048]{1,0:T(8,128)(2,1)} %tok.1, f32[1,2048]{1,0:T(1,128)} %bitcast.11, f32[1,2048]{1,0:T(1,128)} %bitcast.12, f32[1,2048]{1,0:T(1,128)} %bitcast.13, bf16[128,688]{1,0:T(8,128)(2,1)} %copy-done, bf16[128,688]{1,0:T(8,128)(2,1)} %copy-done.1, bf16[128,128]{1,0:T(8,128)(2,1)} %get-tuple-element.10.t1, ...), custom_call_target="tpu_custom_call" | custom-call | tf_op jit(solution)/shard_map/layer/pallas_call | solution.py:540
  203.7 1.9 copy.28
  (6 shorter events, 0.0 us)
Async XLA Ops:
  0.0 3.6 %copy-start.6 = (bf16[128,688]{0,1:T(8,128)(2,1)S(1)}, bf16[128,688]{0,1:T(8,128)(2,1)}, u32[]{:S(2)}) copy-start(bf16[128,688]{0,1:T(8,128)(2,1)} %param.33) | copy-start | bytes 528388
  1.3 2.5 %copy-start.7 = (bf16[128,688]{0,1:T(8,128)(2,1)S(1)}, bf16[128,688]{0,1:T(8,128)(2,1)}, u32[]{:S(2)}) copy-start(bf16[128,688]{0,1:T(8,128)(2,1)} %param.34) | copy-start | bytes 528388
  2.4 1.5 copy-start
  3.6 1.2 copy-start.1
  3.6 1.1 copy-start.4
  3.6 1.2 copy-start.5
  3.8 1.0 copy-start.2
  4.0 1.8 copy-start.3
  4.8 1.0 copy-start.8

commit v2 on v1

--- a/solution.py
+++ b/solution.py
@@ -18,12 +18,15 @@
 NFS = 16
 HID = 688
 HPAD = 768
+BLK = 192
 CH = 384
 SEQ = 1024
 FULL_TILES = HID // 128
 FFN_ROWS = HID + 2 * FULL_TILES * 128 + 128
 MIX_ROWS = 3 * CH
 FFN_CUTS = (0, 528, 1056, 1584, 2096)
+IN_CUTS = (688, 1040, 1392, 1744, 2096)
+DOWN_CUTS = (0, 176, 352, 528, 688)
 MIX_CUTS = (0, 288, 576, 864, 1152)
 
 
@@ -40,10 +43,10 @@
 
 def layer_kernel(
     tok, s1, s2, s3,
-    g1, u1, t1, d1, ri, og, mo, g3, u3, t3, d3,
-    ck, gb, cv, pde,
+    g1, u1, g3, u3, ck, decay, inputs, cdw, extra,
+    d1, ri, og, mo, d3,
     out,
-    w1, w2, w3, xg, hid, ps, pr, po, sb, rb, res, rc, br, sa, sd,
+    w1, w2, w3, xg, hid, ps, pr, po, sb, rb, res, rc, br, sa, sd, gb,
     wl, ws, wr, ags, agr, prs, prr, rss, rsr,
 ):
     fs = lax.axis_index("fs")
@@ -69,15 +72,20 @@
             device_id=dev, device_id_type=MESH,
         )
 
-    def load_ffn(w, g, u, t, d, sem):
+    def load_ffn(w, g, u, d, sem):
         pltpu.make_async_copy(d, w.at[fs, pl.ds(0, HID)], sem).start()
         for j in range(FULL_TILES):
-            cols = pl.ds(j * 128, 128)
-            pltpu.make_async_copy(g.at[:, cols], w.at[fs, pl.ds(HID + j * 128, 128)], sem).start()
-            pltpu.make_async_copy(
-                u.at[:, cols], w.at[fs, pl.ds(HID + (FULL_TILES + j) * 128, 128)], sem
-            ).start()
-        pltpu.make_async_copy(t, w.at[fs, pl.ds(HID + 2 * FULL_TILES * 128, 128)], sem).start()
+            rows = pl.ds(j * 128, 128)
+            w[fs, pl.ds(HID + j * 128, 128), :] = g[rows, :].T
+            w[fs, pl.ds(HID + (FULL_TILES + j) * 128, 128), :] = u[rows, :].T
+        at = FULL_TILES * 128
+        last = jnp.concatenate(
+            [g[at:HID, :], u[at:HID, :], jnp.zeros((128 - 2 * (HID - at), 128), BF16)], axis=0
+        )
+        w[fs, pl.ds(HID + 2 * at, 128), :] = last.T
+
+    def wait_ffn(w, d, sem):
+        pltpu.make_async_copy(d, w.at[fs, pl.ds(0, HID)], sem).wait()
 
     def load_mix(w, sem):
         pltpu.make_async_copy(mo, w.at[fs, pl.ds(0, CH)], sem).start()
@@ -236,9 +244,9 @@
 
         lax.fori_loop(0, ROWS // G, body, 0)
 
-    def ffn_in(w, dx):
-        xd = chip(dx)
-        lhs = xg[pl.ds(2 * xd, 2)].reshape(2 * ROWS, D)
+    def ffn_rows(w, first, count):
+        lhs = xg[pl.ds(first, count)].reshape(count * ROWS, D)
+        dst = pl.ds(first, count)
 
         def tile(at):
             return w[:, pl.ds(pl.multiple_of(at, 16), 128), :].reshape(D, 128)
@@ -248,7 +256,7 @@
             r = jnp.dot(lhs, rhs, preferred_element_type=F32)
             g, u = r[:, :128], r[:, 128:]
             h = (g * sigmoid(g) * u).astype(BF16)
-            hid[pl.ds(2 * xd, 2), :, pl.ds(pl.multiple_of(j * 128, 128), 128)] = h.reshape(2, ROWS, 128)
+            hid[dst, :, pl.ds(pl.multiple_of(j * 128, 128), 128)] = h.reshape(count, ROWS, 128)
             return 0
 
         lax.fori_loop(0, FULL_TILES, body, 0)
@@ -256,7 +264,13 @@
         u = pltpu.roll(r, 128 - (HID - FULL_TILES * 128), 1)
         lane = lax.broadcasted_iota(jnp.int32, r.shape, 1)
         h = jnp.where(lane < HID - FULL_TILES * 128, r * sigmoid(r) * u, 0.0).astype(BF16)
-        hid[pl.ds(2 * xd, 2), :, pl.ds(FULL_TILES * 128, 128)] = h.reshape(2, ROWS, 128)
+        hid[dst, :, pl.ds(FULL_TILES * 128, 128)] = h.reshape(count, ROWS, 128)
+
+    def ffn_in(w, dx):
+        ffn_rows(w, 2 * chip(dx), 2)
+
+    def ffn_in_all(w, i):
+        ffn_rows(w, 4 * i, 4)
 
     def mix_in(dx):
         xd = chip(dx)
@@ -274,6 +288,15 @@
             return 0
 
         lax.fori_loop(0, CH // 128, body, 0)
+
+    def gate_map():
+        a = lax.broadcasted_iota(jnp.int32, (BLK, CH), 0)
+        b = lax.broadcasted_iota(jnp.int32, (BLK, CH), 1)
+        for m, ref in enumerate((decay, inputs)):
+            for k in range(2):
+                place = jnp.where(b == a + k * BLK, 1.0, 0.0).astype(BF16)
+                wide = jnp.dot(ref[k], place, preferred_element_type=F32)
+                gb[pl.ds(k * BLK, BLK), pl.ds(m * CH, CH)] = wide.astype(BF16)
 
     def gates(i):
         at = pl.multiple_of(i * 256, 256)
@@ -287,12 +310,16 @@
             tiles.append(acc.astype(BF16))
         conv = jnp.concatenate(tiles, axis=1)
         both = jnp.dot(conv, gb[...], preferred_element_type=F32)
-        extra = pde[pl.ds(at, 256), :]
+        added = jnp.concatenate(
+            [jnp.broadcast_to(extra[pl.ds(2 * i + k, 1), :], (128, 128)).T for k in range(2)], axis=0
+        )
+        weights = -cdw[...]
+        rates = -8.0 * (jnp.maximum(weights, 0.0) + jnp.log1p(jnp.exp(-jnp.abs(weights))))
         for j in range(CH // 128):
             cols = pl.ds(j * 128, 128)
             rate = sigmoid(both[:, j * 128 : (j + 1) * 128])
             gate = sigmoid(both[:, CH + j * 128 : CH + (j + 1) * 128])
-            log_a = rate * cv[:, cols] + extra
+            log_a = rate * rates[j : j + 1, :] + added
             sa[pl.ds(at, 256), cols] = jnp.exp(log_a)
             sd[pl.ds(at, 256), cols] = (
                 jnp.sqrt(one_minus_exp(2.0 * log_a)) * gate * tiles[j].astype(F32)
@@ -326,14 +353,14 @@
         )
 
         def body(n, _):
-            rhs = jnp.concatenate([w[2 * n, pl.ds(0, depth), :], w[2 * n + 1, pl.ds(0, depth), :]], axis=1)
+            rhs = jnp.concatenate([w[4 * n + i, pl.ds(0, depth), :] for i in range(4)], axis=1)
             r = jnp.dot(lhs, rhs, preferred_element_type=F32).astype(BF16)
-            cols = pl.ds(pl.multiple_of(n * 256, 256), 256)
+            cols = pl.ds(pl.multiple_of(n * 512, 512), 512)
             ps[k, :, cols] = r[:ROWS]
             po[k, :, cols] = r[ROWS:]
             return 0
 
-        lax.fori_loop(0, NFS // 2, body, 0)
+        lax.fori_loop(0, NFS // 4, body, 0)
         rcopy(ps.at[k], pr.at[k], prs.at[l, k], prr.at[l, k], partner).start()
 
     def pair_ready(l, dx):
@@ -416,52 +443,57 @@
             for slot in range(3):
                 ring(l, way, slot).wait_send()
 
-    load_ffn(w1, g1, u1, t1, d1, wl.at[0])
-    load_mix(w2, wl.at[1])
-    load_ffn(w3, g3, u3, t3, d3, wl.at[2])
-
     barrier = pltpu.get_barrier_semaphore()
     peers = [right, left, partner] + [(fs_of(*d), tp) for d in ((0, 1), (0, 3), (1, 0), (3, 0))]
     for dev in peers:
         pl.semaphore_signal(barrier, inc=1, device_id=dev, device_id_type=MESH)
+    load_ffn(w1, g1, u1, d1, wl.at[0])
+    load_mix(w2, wl.at[1])
     first_norm()
-    rc[pl.ds(0, 8), :] = jnp.zeros((8, CH), F32)
     pl.semaphore_wait(barrier, len(peers))
 
-    a1 = weight_steps(0, w1, FFN_CUTS)
-    a2 = weight_steps(1, w2, MIX_CUTS)
-    a3 = weight_steps(2, w3, FFN_CUTS)
-
-    wait_load(w1, wl.at[0])
-    a1[0]()
+    ai = weight_steps(0, w1, IN_CUTS)
+    ad = weight_steps(1, w1, DOWN_CUTS)
+    a2 = weight_steps(2, w2, MIX_CUTS)
+    a3 = weight_steps(3, w3, FFN_CUTS)
+
+    ai[0]()
     start, forward, near, far, ready, drain = gather_steps(0)
     start()
-    a1[1]()
-    a1[2]()
+    load_ffn(w3, g3, u3, d3, wl.at[2])
+    gate_map()
+    rc[pl.ds(0, 8), :] = jnp.zeros((8, CH), F32)
+    wait_ffn(w1, d1, wl.at[0])
+    wait_load(w2, wl.at[1])
+    wait_ffn(w3, d3, wl.at[2])
+    ai[1]()
+    ai[2]()
     forward()
-    a1[3]()
+    ai[3]()
     near()
-    a1[4]()
+    ai[4]()
     far()
-    a1[5]()
+    ai[5]()
     for dx in (0, 3, 1, 2):
         ready(dx)
     drain()
-    wait_load(w2, wl.at[1])
-    wait_load(w3, wl.at[2])
-    a1[6]()
-    a1[7]()
+    ai[6]()
+    ai[7]()
+    ad[0]()
+    ai[8]()
+    ad[1]()
+    ad[2]()
+    ffn_in_all(w1, 0)
+    ad[3]()
+    ad[4]()
+    ffn_in_all(w1, 1)
+    for k in (5, 6, 7):
+        ad[k]()
     a2[0]()
-    a1[8]()
-    for i, dx in enumerate((2, 1, 3, 0)):
-        ffn_in(w1, dx)
-        if i == 1:
-            a2[1]()
-        if i == 2:
-            a2[2]()
-        if i == 3:
-            a2[3]()
-    reduce(0, w1, HPAD, tok, 0.5, s2, res, [[a2[4]], [a2[5]], [a2[6]], [a2[7], a3[0]]])
+    ad[8]()
+    a2[1]()
+    a2[2]()
+    reduce(0, w1, HPAD, tok, 0.5, s2, res, [[a2[3]], [a2[4]], [a2[5], a2[6]], [a2[7], a3[0]]])
 
     start, forward, near, far, ready, drain = gather_steps(1)
     start()
@@ -508,26 +540,10 @@
     ffn_in(w3, 2)
     drain()
     reduce(2, w3, HPAD, res, 0.5, None, out, [])
-    a1[9]()
+    ai[9]()
+    ad[9]()
     a2[9]()
     a3[9]()
-
-
-def gate_map(decay, inputs):
-    def diagonal(b):
-        return jnp.concatenate(
-            [jnp.pad(b[0], ((0, 0), (0, 192))), jnp.pad(b[1], ((0, 0), (192, 0)))], axis=0
-        )
-
-    return jnp.concatenate([diagonal(decay), diagonal(inputs)], axis=1)
-
-
-def tail(gate, up):
-    at = FULL_TILES * 128
-    left = gate.shape[1] - at
-    return jnp.concatenate(
-        [gate[:, at:], up[:, at:], jnp.zeros((gate.shape[0], 128 - 2 * left), gate.dtype)], axis=1
-    )
 
 
 def shards(
@@ -540,7 +556,7 @@
     return pl.pallas_call(
         layer_kernel,
         out_shape=jax.ShapeDtypeStruct((ROWS, D), BF16),
-        in_specs=[vmem] * 4 + [hbm] * 11 + [vmem] * 4,
+        in_specs=[vmem] * 13 + [hbm] * 5,
         out_specs=vmem,
         scratch_shapes=[
             pltpu.VMEM((NFS, FFN_ROWS, 128), BF16),
@@ -558,9 +574,10 @@
             pltpu.VMEM((SEQ, CH), BF16),
             pltpu.VMEM((SEQ, CH), F32),
             pltpu.VMEM((SEQ, CH), F32),
+            pltpu.VMEM((CH, 2 * CH), BF16),
             dma((3,)),
-            dma((3, 40)),
-            dma((3, 40)),
+            dma((4, 40)),
+            dma((4, 40)),
             dma((3, 10)),
             dma((3, 10)),
             dma((3, 4)),
@@ -574,9 +591,8 @@
         name="layer",
     )(
         tokens, row(s1), row(s2), row(s3),
-        g1, u1, tail(g1, u1), d1, ri, og, mo, g3, u3, tail(g3, u3), d3,
-        ck, gate_map(decay, inputs), row(-8.0 * jax.nn.softplus(-cdw)),
-        jnp.broadcast_to(extra[:, None], (SEQ, 128)),
+        g1.T, u1.T, g3.T, u3.T, ck, decay, inputs, cdw.reshape(3, 128), extra.reshape(8, 128),
+        d1, ri, og, mo, d3,
     )
 
 

time: 206 us -> 192 us (0.932)
  Pallas kernels: 197 us -> 190 us
  local copies, waits for them, and re-layouts: 6.11 us -> 1.88 us
  other arithmetic: 2.35 us -> 0 us
    pallas_call x1, Pallas kernels: 197 us -> 190 us  [shards(): pl.pallas_call(layer_kernel, out_shape=jax.ShapeDtypeStruct((ROWS, D), BF...]
    unnamed x23 -> x1, local copies, waits for them, and re-layouts: 4.46 us -> 1.88 us
where the time goes in v2:
time: 192 us
  Pallas kernels  190 us (99%)
    pallas_call x1, Pallas kernels, shards(): pl.pallas_call(layer_kernel, out_shape=jax.ShapeDtypeStruct((ROWS, D), BF...  190 us

profile of v2, /device:TPU:1, one launch (start us, length us, event | category | flops | bytes accessed | tf_op | source)
XLA Modules:
  0.0 191.7 jit_solution(7383872747370503277)
XLA Ops:
  0.0 189.8 %layer.1 = bf16[128,2048]{1,0:T(8,128)(2,1)} custom-call(bf16[128,2048]{1,0:T(8,128)(2,1)} %tok.1, f32[1,2048]{1,0:T(1,128)} %bitcast.13, f32[1,2048]{1,0:T(1,128)} %bitcast.14, f32[1,2048]{1,0:T(1,128)} %bitcast.15, bf16[688,128]{1,0:T(8,128)(2,1)} %bitcast.9, bf16[688,128]{1,0:T(8,128)(2,1)} %bitcast.10, bf16[688,128]{1,0:T(8,128)(2,1)} %bitcast.11, ...), custom_call_target="tpu_custom_call" | custom-call | tf_op jit(solution)/shard_map/layer/pallas_call | solution.py:556
  189.8 1.9 copy.20

commit v3 on v2

v3 whole, which is shorter than its diff:
```python
import functools

import jax
import jax.numpy as jnp
from jax import lax
from jax.experimental import pallas as pl
from jax.experimental.pallas import tpu as pltpu
from jax.sharding import PartitionSpec as P

EPS = 1e-06
MESH = pl.DeviceIdType.MESH
F32 = jnp.float32
BF16 = jnp.bfloat16

ROWS = 128
HALF = ROWS // 2
QUART = ROWS // 4
D = 2048
NFS = 16
HID = 688
HPAD = 768
BLK = 192
CH = 384
SEQ = 1024
FULL_TILES = HID // 128
FFN_ROWS = HID + 2 * FULL_TILES * 128 + 128
MIX_ROWS = 3 * CH
FFN_CUTS = (0, 528, 1056, 1584, 2096)
IN_CUTS = (688, 1040, 1392, 1744, 2096)
DOWN_CUTS = (0, 176, 352, 528, 688)
MIX_CUTS = (0, 288, 576, 864, 1152)


def sigmoid(v):
    return 1.0 / (1.0 + jnp.exp(-v))


def one_minus_square(a, v):
    series = 1.0 / 120.0
    for term in (1.0 / 24.0, 1.0 / 6.0, 0.5, 1.0):
        series = term + v * series
    return jnp.where(v > -0.0625, -v * series, 1.0 - a * a)


def layer_kernel(
    tok, s1, s2, s3,
    g1, u1, g3, u3, ck, decay, inputs, cdw, extra,
    d1, ri, og, mo, d3,
    out,
    w1, w2, w3, xg, hid, ps, pr, po, sb, rb, res, rc, br, sa, sd, gb, cv, pde,
    wl, ws, wr, ags, agr, prs, prr, rss, rsr,
):
    fs = lax.axis_index("fs")
    tp = lax.axis_index("tp")
    z, y = fs // 4, fs % 4
    x, c = tp // 2, tp % 2

    def chip(dx):
        return (x + dx) % 4

    def dev_x(dx):
        return (fs, chip(dx) * 2 + c)

    partner = (fs, x * 2 + (1 - c))
    right, left = dev_x(1), dev_x(3)

    def fs_of(dz, dy):
        return ((z + dz) % 4) * 4 + (y + dy) % 4

    def rcopy(src, dst, ssem, rsem, dev):
        return pltpu.make_async_remote_copy(
            src_ref=src, dst_ref=dst, send_sem=ssem, recv_sem=rsem,
            device_id=dev, device_id_type=MESH,
        )

    def load_ffn(w, g, u, d, sem):
        pltpu.make_async_copy(d, w.at[fs, pl.ds(0, HID)], sem).start()
        for j in range(FULL_TILES):
            rows = pl.ds(j * 128, 128)
            w[fs, pl.ds(HID + j * 128, 128), :] = g[rows, :].T
            w[fs, pl.ds(HID + (FULL_TILES + j) * 128, 128), :] = u[rows, :].T
        at = FULL_TILES * 128
        last = jnp.concatenate(
            [g[at:HID, :], u[at:HID, :], jnp.zeros((128 - 2 * (HID - at), 128), BF16)], axis=0
        )
        w[fs, pl.ds(HID + 2 * at, 128), :] = last.T

    def wait_ffn(w, d, sem):
        pltpu.make_async_copy(d, w.at[fs, pl.ds(0, HID)], sem).wait()

    def load_mix(w, sem):
        pltpu.make_async_copy(mo, w.at[fs, pl.ds(0, CH)], sem).start()
        for j in range(CH // 128):
            cols = pl.ds(j * 128, 128)
            pltpu.make_async_copy(ri.at[:, cols], w.at[fs, pl.ds(CH + j * 128, 128)], sem).start()
            pltpu.make_async_copy(og.at[:, cols], w.at[fs, pl.ds(2 * CH + j * 128, 128)], sem).start()

    def wait_load(w, sem):
        pltpu.make_async_copy(w.at[fs], w.at[fs], sem).wait()

    def weight_steps(n, w, cuts):
        def block(h, dp, dq):
            return fs_of(dq, dp) if h == 0 else fs_of(dp, dq)

        def rows(h, part):
            lo, mid, hi = cuts[2 * h], cuts[2 * h + 1], cuts[2 * h + 2]
            a, b = {"all": (lo, hi), "first": (lo, mid), "second": (mid, hi)}[part]
            return pl.ds(a, b - a)

        def desc(h, dp, dq, part, k, to):
            ref = w.at[block(h, dp, dq), rows(h, part)]
            return rcopy(ref, ref, ws.at[n], wr.at[n % 2, 20 * h + k], (block(h, *to), tp))

        def send(*a):
            desc(*a).start()

        def recv(h, dp, dq, part, k):
            desc(h, dp, dq, part, k, (0, 0)).wait_recv()

        offs = (0, 3, 1, 2)

        def start():
            for h in (0, 1):
                send(h, 0, 0, "all", 0, (1, 0))
                send(h, 0, 0, "all", 1, (3, 0))
            for h in (0, 1):
                send(h, 0, 0, "all", 4, (0, 1))
                send(h, 0, 0, "all", 5, (0, 3))

        def across(h, j):
            send(h, offs[j], 0, "all", 4 + 4 * j, (0, 1))
            send(h, offs[j], 0, "all", 5 + 4 * j, (0, 3))

        def near(j):
            for h in (0, 1):
                recv(h, offs[j], 0, "all", j - 1)
                if j == 1:
                    send(h, 3, 0, "first", 2, (1, 0))
                else:
                    send(h, 1, 0, "second", 3, (3, 0))
            for h in (0, 1):
                across(h, j)

        def far():
            for h in (0, 1):
                recv(h, 2, 0, "first", 2)
                recv(h, 2, 0, "second", 3)
                across(h, 3)

        def forward(j):
            for h in (0, 1):
                recv(h, offs[j], 3, "all", 4 + 4 * j)
                send(h, offs[j], 3, "first", 6 + 4 * j, (0, 1))
            for h in (0, 1):
                recv(h, offs[j], 1, "all", 5 + 4 * j)
                send(h, offs[j], 1, "second", 7 + 4 * j, (0, 3))

        def last():
            for j in range(4):
                for h in (0, 1):
                    recv(h, offs[j], 2, "first", 6 + 4 * j)
                    recv(h, offs[j], 2, "second", 7 + 4 * j)

        def drain():
            sent = w.at[pl.ds(0, 15), pl.ds(cuts[0], cuts[4] - cuts[0])]
            pltpu.make_async_copy(sent, sent, ws.at[n]).wait()

        return [
            start,
            functools.partial(near, 1),
            functools.partial(near, 2),
            functools.partial(forward, 0),
            far,
            functools.partial(forward, 1),
            functools.partial(forward, 2),
            functools.partial(forward, 3),
            last,
            drain,
        ]

    def gather_steps(l, m):
        lo, hi, both = pl.ds(HALF * m, QUART), pl.ds(HALF * m + QUART, QUART), pl.ds(HALF * m, HALF)
        def blk(dx, same=True):
            return chip(dx) * 2 + (c if same else 1 - c)

        def send(ref, k, dev):
            rcopy(ref, ref, ags.at[m], agr.at[m, k], dev).start()

        def recv(ref, k):
            rcopy(ref, ref, ags.at[m], agr.at[m, k], partner).wait_recv()

        def start():
            send(xg.at[blk(0), lo], 1, right)
            send(xg.at[blk(0), hi], 2, left)
            send(xg.at[blk(0), hi], 3, right)
            send(xg.at[blk(0), lo], 4, left)
            send(xg.at[blk(0), both], 0, partner)

        def forward():
            recv(xg.at[blk(3), lo], 1)
            send(xg.at[blk(3), lo], 5, right)
            recv(xg.at[blk(1), hi], 2)
            send(xg.at[blk(1), hi], 6, left)

        def near():
            recv(xg.at[blk(3), hi], 3)
            send(xg.at[blk(3), both], 7, partner)
            recv(xg.at[blk(1), lo], 4)
            send(xg.at[blk(1), both], 8, partner)

        def far():
            recv(xg.at[blk(2), lo], 5)
            recv(xg.at[blk(2), hi], 6)
            send(xg.at[blk(2), both], 9, partner)

        def ready():
            for dx, k in ((0, 0), (3, 7), (1, 8), (2, 9)):
                recv(xg.at[blk(dx, False), both], k)
            sent = xg.at[pl.ds(0, 7), both]
            pltpu.make_async_copy(sent, sent, ags.at[m]).wait()

        return start, forward, near, far, ready

    def normed(values, scale):
        square = jnp.mean(values * values, axis=-1, keepdims=True)
        return (values * lax.rsqrt(square + EPS) * scale[...]).astype(BF16)

    G = 16

    def first_norm():
        def body(i, _):
            r = pl.ds(pl.multiple_of(i * G, G), G)
            xg[tp, r, :] = normed(tok[r, :].astype(F32), s1)
            return 0

        lax.fori_loop(0, ROWS // G, body, 0)

    def half_rows(m):
        return xg[:, pl.ds(HALF * m, HALF), :].reshape(8 * HALF, D)

    def ffn_in(w, m, between=()):
        lhs = half_rows(m)
        dst = pl.ds(HALF * m, HALF)

        def tile(at):
            return w[:, pl.ds(pl.multiple_of(at, 16), 128), :].reshape(D, 128)

        def body(j, _):
            rhs = jnp.concatenate([tile(HID + j * 128), tile(HID + (FULL_TILES + j) * 128)], axis=1)
            r = jnp.dot(lhs, rhs, preferred_element_type=F32)
            g, u = r[:, :128], r[:, 128:]
            h = (g * sigmoid(g) * u).astype(BF16)
            hid[:, dst, pl.ds(pl.multiple_of(j * 128, 128), 128)] = h.reshape(8, HALF, 128)
            return 0

        lax.fori_loop(0, 2, body, 0)
        run(between[:1])
        lax.fori_loop(2, 4, body, 0)
        run(between[1:])
        lax.fori_loop(4, FULL_TILES, body, 0)
        r = jnp.dot(lhs, tile(HID + 2 * FULL_TILES * 128), preferred_element_type=F32)
        u = pltpu.roll(r, 128 - (HID - FULL_TILES * 128), 1)
        lane = lax.broadcasted_iota(jnp.int32, r.shape, 1)
        h = jnp.where(lane < HID - FULL_TILES * 128, r * sigmoid(r) * u, 0.0).astype(BF16)
        hid[:, dst, pl.ds(FULL_TILES * 128, 128)] = h.reshape(8, HALF, 128)

    def mix_in(m):
        lhs = half_rows(m)

        def tile(at):
            return w2[:, pl.ds(pl.multiple_of(at, 16), 128), :].reshape(D, 128)

        def body(j, _):
            rhs = jnp.concatenate([tile(CH + j * 128), tile(2 * CH + j * 128)], axis=1)
            r = jnp.dot(lhs, rhs, preferred_element_type=F32).astype(BF16)
            cols = pl.ds(pl.multiple_of(j * 128, 128), 128)
            rc[:, pl.ds(8 + HALF * m, HALF), cols] = r[:, :128].astype(F32).reshape(8, HALF, 128)
            br[:, pl.ds(HALF * m, HALF), cols] = r[:, 128:].reshape(8, HALF, 128)
            return 0

        lax.fori_loop(0, CH // 128, body, 0)

    def gate_map():
        a = lax.broadcasted_iota(jnp.int32, (BLK, CH), 0)
        b = lax.broadcasted_iota(jnp.int32, (BLK, CH), 1)
        for m, ref in enumerate((decay, inputs)):
            for k in range(2):
                place = jnp.where(b == a + k * BLK, 1.0, 0.0).astype(BF16)
                wide = jnp.dot(ref[k], place, preferred_element_type=F32)
                gb[pl.ds(k * BLK, BLK), pl.ds(m * CH, CH)] = wide.astype(BF16)

    def halo():
        rc[0, pl.ds(0, 8), :] = jnp.zeros((8, CH), F32)
        for t in range(1, 8):
            rc[t, pl.ds(0, 8), :] = rc[t - 1, pl.ds(ROWS, 8), :]

    def gate_rates():
        weights = -cdw[...]
        cv[...] = -8.0 * (jnp.maximum(weights, 0.0) + jnp.log1p(jnp.exp(-jnp.abs(weights))))
        for t in range(8):
            pde[t] = jnp.broadcast_to(extra[pl.ds(t, 1), :], (128, 128)).T

    def gates(first, blocks, base, count):
        t = pl.ds(first, blocks)
        size = blocks * count
        dst = pl.ds(base, count)
        tiles = []
        for j in range(CH // 128):
            cols = pl.ds(j * 128, 128)
            rows = []
            for k in range(blocks):
                window = rc[first + k, pl.ds(base, count + 8), cols]
                acc = window[8:] * ck[3:4, cols]
                for s in (1, 2, 3):
                    acc = acc + pltpu.roll(window, s, 0)[8:] * ck[3 - s : 4 - s, cols]
                rows.append(acc)
            tiles.append(jnp.concatenate(rows, axis=0).astype(BF16))
        conv = jnp.concatenate(tiles, axis=1)
        maps = jnp.dot(conv, gb[...], preferred_element_type=F32)
        added = pde[t, dst, :].reshape(size, 128)
        for j in range(CH // 128):
            cols = pl.ds(j * 128, 128)
            rate = sigmoid(maps[:, j * 128 : (j + 1) * 128])
            gate = sigmoid(maps[:, CH + j * 128 : CH + (j + 1) * 128])
            log_a = rate * cv[j : j + 1, :] + added
            a = jnp.exp(log_a)
            drive = jnp.sqrt(one_minus_square(a, 2.0 * log_a)) * gate * tiles[j].astype(F32)
            sa[t, dst, cols] = a.reshape(blocks, count, 128)
            sd[t, dst, cols] = drive.reshape(blocks, count, 128)

    def gates_half(m):
        def body(i, _):
            gates(4 * i, 4, HALF * m, HALF)
            return 0

        lax.fori_loop(0, 2, body, 0)

    T = 64

    def scan_chunk(i, carry):
        r = pl.ds(pl.multiple_of((i % 2) * T, T), T)
        a, b = sa[i // 2, r, :], sd[i // 2, r, :]
        row = lax.broadcasted_iota(jnp.int32, (T, CH), 0)
        s = 1
        while s < T:
            here = row >= s
            b = a * jnp.where(here, pltpu.roll(b, s, 0), 0.0) + b
            a = a * jnp.where(here, pltpu.roll(a, s, 0), 1.0)
            s *= 2
        state = b + a * carry
        v = br[i // 2, r, :].astype(F32)
        gelu = 0.5 * v * (1.0 + jnp.tanh(0.7978845608028654 * (v + 0.044715 * v * v * v)))
        hid[i // 2, r, pl.ds(0, CH)] = (gelu * state).astype(BF16)
        return state[T - 1 : T, :]

    SLOT = {2: 0, 1: 1, 3: 2, 0: 3}

    def pair_copy(l, m, k):
        return rcopy(ps.at[m, k], pr.at[m, k], prs.at[m], prr.at[m, k], partner)

    def project(l, w, depth, m, pair):
        rows = pl.ds(HALF * m, HALF)
        k0 = SLOT[pair[0]]
        lhs = jnp.concatenate(
            [hid[2 * chip(dx) + 1 - c, rows, pl.ds(0, depth)] for dx in pair]
            + [hid[2 * chip(dx) + c, rows, pl.ds(0, depth)] for dx in pair],
            axis=0,
        )

        def body(n, _):
            rhs = jnp.concatenate([w[4 * n + i, pl.ds(0, depth), :] for i in range(4)], axis=1)
            r = jnp.dot(lhs, rhs, preferred_element_type=F32).astype(BF16)
            cols = pl.ds(pl.multiple_of(n * 512, 512), 512)
            ps[m, pl.ds(k0, 2), :, cols] = r[:ROWS].reshape(2, HALF, 512)
            po[m, pl.ds(k0, 2), :, cols] = r[ROWS:].reshape(2, HALF, 512)
            return 0

        lax.fori_loop(0, NFS // 4, body, 0)
        pair_copy(l, m, k0).start()
        pair_copy(l, m, k0 + 1).start()

    def ring(l, m, way, slot):
        return rcopy(
            sb.at[m, way, slot], rb.at[m, way, slot], rss.at[m],
            rsr.at[m, way, slot], (right, left)[way],
        )

    def both(m, k, r):
        return po[m, k, r, :].astype(F32) + pr[m, k, r, :].astype(F32)

    def post(l, m, way, slot, dx, base, extra=None):
        def body(i, _):
            at = pl.multiple_of(i * G, G)
            v = both(m, SLOT[dx], pl.ds(base + at, G))
            if extra is not None:
                v = v + rb[m, way, extra, pl.ds(at, G), :].astype(F32)
            sb[m, way, slot, pl.ds(at, G), :] = v.astype(BF16)
            return 0

        lax.fori_loop(0, QUART // G, body, 0)
        ring(l, m, way, slot).start()

    def post_first(l, m):
        pair_copy(l, m, SLOT[2]).wait_recv()
        post(l, m, 0, 0, 2, 0)
        post(l, m, 1, 0, 2, QUART)
        pair_copy(l, m, SLOT[1]).wait_recv()
        post(l, m, 0, 1, 1, QUART)

    def post_second(l, m):
        pair_copy(l, m, SLOT[3]).wait_recv()
        post(l, m, 1, 1, 3, 0)

    def send_half(l, w, depth, m, between=()):
        project(l, w, depth, m, (2, 1))
        run(between)
        post_first(l, m)
        project(l, w, depth, m, (3, 0))
        post_second(l, m)

    def post_ring(l, m):
        ring(l, m, 0, 0).wait_recv()
        post(l, m, 0, 2, 1, 0, extra=0)
        ring(l, m, 1, 0).wait_recv()
        post(l, m, 1, 2, 3, QUART, extra=0)

    def finish(l, m, before, weight, scale, result):
        pair_copy(l, m, SLOT[0]).wait_recv()
        for way in (0, 1):
            ring(l, m, way, 1).wait_recv()
            ring(l, m, way, 2).wait_recv()
        for base, a, b in ((0, 2, 1), (QUART, 1, 2)):

            def body(i, _):
                at = pl.multiple_of(i * G, G)
                r = pl.ds(HALF * m + base + at, G)
                v = both(m, SLOT[0], pl.ds(base + at, G))
                v = v + rb[m, 0, a, pl.ds(at, G), :].astype(F32) + rb[m, 1, b, pl.ds(at, G), :].astype(F32)
                v = (before[r, :].astype(F32) + weight * v).astype(BF16)
                result[r, :] = v
                if scale is not None:
                    xg[tp, r, :] = normed(v.astype(F32), scale)
                return 0

            lax.fori_loop(0, QUART // G, body, 0)
        pltpu.make_async_copy(ps.at[m], ps.at[m], prs.at[m]).wait()
        pltpu.make_async_copy(sb.at[m], sb.at[m], rss.at[m]).wait()

    def run(steps):
        for s in steps:
            s()

    barrier = pltpu.get_barrier_semaphore()
    peers = [right, left, partner] + [(fs_of(*d), tp) for d in ((0, 1), (0, 3), (1, 0), (3, 0))]
    for dev in peers:
        pl.semaphore_signal(barrier, inc=1, device_id=dev, device_id_type=MESH)
    load_ffn(w1, g1, u1, d1, wl.at[0])
    load_mix(w2, wl.at[1])
    first_norm()
    pl.semaphore_wait(barrier, len(peers))

    ai = weight_steps(0, w1, IN_CUTS)
    ad = weight_steps(1, w1, DOWN_CUTS)
    a2 = weight_steps(2, w2, MIX_CUTS)
    a3 = weight_steps(3, w3, FFN_CUTS)

    ai[0]()
    ga, gc = gather_steps(0, 0), gather_steps(0, 1)
    ga[0]()
    gc[0]()
    load_ffn(w3, g3, u3, d3, wl.at[2])
    gate_map()
    gate_rates()
    rc[:, pl.ds(0, 8), :] = jnp.zeros((8, 8, CH), F32)
    wait_ffn(w1, d1, wl.at[0])
    wait_load(w2, wl.at[1])
    wait_ffn(w3, d3, wl.at[2])
    ai[1]()
    ai[2]()
    ga[1]()
    gc[1]()
    ai[3]()
    ga[2]()
    gc[2]()
    ai[4]()
    ga[3]()
    gc[3]()
    ai[5]()
    ga[4]()
    gc[4]()
    ai[6]()
    ai[7]()
    ad[0]()
    ai[8]()
    ad[1]()
    ad[2]()
    ffn_in(w1, 0, (ad[3], ad[4]))
    ad[5]()
    ffn_in(w1, 1, (ad[6], ad[7]))
    a2[0]()
    ad[8]()

    send_half(0, w1, HPAD, 0)
    run(a2[1:3])
    project(0, w1, HPAD, 1, (2, 1))
    post_ring(0, 0)
    post_first(0, 1)
    project(0, w1, HPAD, 1, (3, 0))
    post_second(0, 1)
    a2[3]()
    ga, gc = gather_steps(1, 0), gather_steps(1, 1)
    finish(0, 0, tok, 0.5, s2, res)
    a2[4]()
    post_ring(0, 1)
    ga[0]()
    run(a2[5:7])
    finish(0, 1, tok, 0.5, s2, res)
    ga[1]()
    gc[0]()
    a2[7]()
    a3[0]()
    ga[2]()
    ga[3]()
    a2[8]()
    ga[4]()
    mix_in(0)
    gc[1]()
    gates_half(0)
    gc[2]()
    gc[3]()
    gc[4]()
    mix_in(1)
    halo()
    gates_half(1)
    gates(0, 8, 0, 8)
    run(a3[1:3])
    lax.fori_loop(0, SEQ // T, scan_chunk, jnp.zeros((1, CH), F32))

    send_half(1, w2, CH, 0)
    a3[3]()
    project(1, w2, CH, 1, (2, 1))
    post_ring(1, 0)
    post_first(1, 1)
    project(1, w2, CH, 1, (3, 0))
    post_second(1, 1)
    a3[4]()
    ga, gc = gather_steps(2, 0), gather_steps(2, 1)
    finish(1, 0, res, 1.0, s3, res)
    post_ring(1, 1)
    ga[0]()
    a3[5]()
    finish(1, 1, res, 1.0, s3, res)
    a3[6]()
    ga[1]()
    gc[0]()
    a3[7]()
    ga[2]()
    ga[3]()
    a3[8]()
    ga[4]()
    ffn_in(w3, 0, (gc[1],))
    send_half(2, w3, HPAD, 0)
    gc[2]()
    gc[3]()
    gc[4]()
    ffn_in(w3, 1, (lambda: post_ring(2, 0),))
    project(2, w3, HPAD, 1, (2, 1))
    post_first(2, 1)
    project(2, w3, HPAD, 1, (3, 0))
    post_second(2, 1)
    finish(2, 0, res, 0.5, None, out)
    ai[9]()
    ad[9]()
    a2[9]()
    a3[9]()
    post_ring(2, 1)
    finish(2, 1, res, 0.5, None, out)


def shards(
    tokens, s1, g1, u1, d1, s2, ri, og, ck, decay, inputs, cdw, extra, mo, s3, g3, u3, d3
):
    vmem = pl.BlockSpec(memory_space=pltpu.VMEM)
    hbm = pl.BlockSpec(memory_space=pl.ANY)
    row = lambda v: v.reshape(1, -1)
    dma = pltpu.SemaphoreType.DMA
    return pl.pallas_call(
        layer_kernel,
        out_shape=jax.ShapeDtypeStruct((ROWS, D), BF16),
        in_specs=[vmem] * 13 + [hbm] * 5,
        out_specs=vmem,
        scratch_shapes=[
            pltpu.VMEM((NFS, FFN_ROWS, 128), BF16),
            pltpu.VMEM((NFS, MIX_ROWS, 128), BF16),
            pltpu.VMEM((NFS, FFN_ROWS, 128), BF16),
            pltpu.VMEM((8, ROWS, D), BF16),
            pltpu.VMEM((8, ROWS, HPAD), BF16),
            pltpu.VMEM((2, 4, HALF, D), BF16),
            pltpu.VMEM((2, 4, HALF, D), BF16),
            pltpu.VMEM((2, 4, HALF, D), BF16),
            pltpu.VMEM((2, 2, 3, QUART, D), BF16),
            pltpu.VMEM((2, 2, 3, QUART, D), BF16),
            pltpu.VMEM((ROWS, D), BF16),
            pltpu.VMEM((8, ROWS + 8, CH), F32),
            pltpu.VMEM((8, ROWS, CH), BF16),
            pltpu.VMEM((8, ROWS, CH), F32),
            pltpu.VMEM((8, ROWS, CH), F32),
            pltpu.VMEM((CH, 2 * CH), BF16),
            pltpu.VMEM((3, 128), F32),
            pltpu.VMEM((8, 128, 128), F32),
            dma((3,)),
            dma((4,)),
            dma((2, 40)),
            dma((2,)),
            dma((2, 10)),
            dma((2,)),
            dma((2, 4)),
            dma((2,)),
            dma((2, 2, 3)),
        ],
        compiler_params=pltpu.CompilerParams(
            collective_id=0, has_side_effects=True, vmem_limit_bytes=60 * 1024 * 1024
        ),
        name="layer",
    )(
        tokens, row(s1), row(s2), row(s3),
        g1.T, u1.T, g3.T, u3.T, ck, decay, inputs, cdw.reshape(3, 128), extra.reshape(8, 128),
        d1, ri, og, mo, d3,
    )


def solution(mesh):
    in_specs = (
        P(("fs", "tp"), None), P(), P("fs", "tp"), P("fs", "tp"), P("tp", "fs"),
        P(), P("fs", "tp"), P("fs", "tp"), P(None, "tp"), P("tp", None, None),
        P("tp", None, None), P("tp"), P("fs"), P("tp", "fs"), P(),
        P("fs", "tp"), P("fs", "tp"), P("tp", "fs"),
    )
    out_specs = P(("fs", "tp"), None)
    return jax.shard_map(shards, mesh=mesh, in_specs=in_specs, out_specs=out_specs, check_vma=False)
```

time: 192 us -> 173 us (0.901)
  Pallas kernels: 190 us -> 171 us
    pallas_call x1, Pallas kernels: 190 us -> 171 us  [shards(): pl.pallas_call(layer_kernel, out_shape=jax.ShapeDtypeStruct((ROWS, D), BF...]
where the time goes in v3:
time: 173 us
  Pallas kernels  171 us (99%)
  local copies, waits for them, and re-layouts  1.88 us (1%)
    pallas_call x1, Pallas kernels, shards(): pl.pallas_call(layer_kernel, out_shape=jax.ShapeDtypeStruct((ROWS, D), BF...  171 us

profile of v3, /device:TPU:1, one launch (start us, length us, event | category | flops | bytes accessed | tf_op | source)
XLA Modules:
  0.0 172.7 jit_solution(1081713980170937006)
XLA Ops:
  0.0 170.8 %layer.1 = bf16[128,2048]{1,0:T(8,128)(2,1)} custom-call(bf16[128,2048]{1,0:T(8,128)(2,1)} %tok.1, f32[1,2048]{1,0:T(1,128)} %bitcast.13, f32[1,2048]{1,0:T(1,128)} %bitcast.14, f32[1,2048]{1,0:T(1,128)} %bitcast.15, bf16[688,128]{1,0:T(8,128)(2,1)} %bitcast.9, bf16[688,128]{1,0:T(8,128)(2,1)} %bitcast.10, bf16[688,128]{1,0:T(8,128)(2,1)} %bitcast.11, ...), custom_call_target="tpu_custom_call" | custom-call | tf_op jit(solution)/shard_map/layer/pallas_call | solution.py:587
  170.8 1.9 %copy.20 = bf16[128,2048]{1,0:T(8,128)(2,1)} copy(bf16[128,2048]{1,0:T(8,128)(2,1)} %layer.1) | data formatting | bytes 1048576

commit v4 on v3

--- a/solution.py
+++ b/solution.py
@@ -43,12 +43,12 @@
 
 
 def layer_kernel(
-    tok, s1, s2, s3,
-    g1, u1, g3, u3, ck, decay, inputs, cdw, extra,
-    d1, ri, og, mo, d3,
-    out,
+    tok_in, s1_in, s2_in, s3_in, g1_in, u1_in, g3_in, u3_in, ck_in, decay_in, inputs_in, cdw_in,
+    extra_in, d1, ri, og, mo, d3,
+    out_hbm,
+    out, tok, s1, s2, s3, g1, u1, g3, u3, ck, decay, inputs, cdw, extra,
     w1, w2, w3, xg, hid, ps, pr, po, sb, rb, res, rc, br, sa, sd, gb, cv, pde,
-    wl, ws, wr, ags, agr, prs, prr, rss, rsr,
+    fetched, leave, wl, ws, wr, ags, agr, prs, prr, rss, rsr,
 ):
     fs = lax.axis_index("fs")
     tp = lax.axis_index("tp")
@@ -73,8 +73,7 @@
             device_id=dev, device_id_type=MESH,
         )
 
-    def load_ffn(w, g, u, d, sem):
-        pltpu.make_async_copy(d, w.at[fs, pl.ds(0, HID)], sem).start()
+    def load_ffn(w, g, u):
         for j in range(FULL_TILES):
             rows = pl.ds(j * 128, 128)
             w[fs, pl.ds(HID + j * 128, 128), :] = g[rows, :].T
@@ -253,11 +252,11 @@
             hid[:, dst, pl.ds(pl.multiple_of(j * 128, 128), 128)] = h.reshape(8, HALF, 128)
             return 0
 
-        lax.fori_loop(0, 2, body, 0)
+        lax.fori_loop(0, 2, body, 0, unroll=True)
         run(between[:1])
-        lax.fori_loop(2, 4, body, 0)
+        lax.fori_loop(2, 4, body, 0, unroll=True)
         run(between[1:])
-        lax.fori_loop(4, FULL_TILES, body, 0)
+        body(4, 0)
         r = jnp.dot(lhs, tile(HID + 2 * FULL_TILES * 128), preferred_element_type=F32)
         u = pltpu.roll(r, 128 - (HID - FULL_TILES * 128), 1)
         lane = lax.broadcasted_iota(jnp.int32, r.shape, 1)
@@ -278,7 +277,7 @@
             br[:, pl.ds(HALF * m, HALF), cols] = r[:, 128:].reshape(8, HALF, 128)
             return 0
 
-        lax.fori_loop(0, CH // 128, body, 0)
+        lax.fori_loop(0, CH // 128, body, 0, unroll=True)
 
     def gate_map():
         a = lax.broadcasted_iota(jnp.int32, (BLK, CH), 0)
@@ -343,9 +342,13 @@
         row = lax.broadcasted_iota(jnp.int32, (T, CH), 0)
         s = 1
         while s < T:
-            here = row >= s
-            b = a * jnp.where(here, pltpu.roll(b, s, 0), 0.0) + b
-            a = a * jnp.where(here, pltpu.roll(a, s, 0), 1.0)
+            if s < 8:
+                here = row >= s
+                b = a * jnp.where(here, pltpu.roll(b, s, 0), 0.0) + b
+                a = a * jnp.where(here, pltpu.roll(a, s, 0), 1.0)
+            else:
+                b = jnp.concatenate([b[:s], a[s:] * b[:-s] + b[s:]], axis=0)
+                a = jnp.concatenate([a[:s], a[s:] * a[:-s]], axis=0)
             s *= 2
         state = b + a * carry
         v = br[i // 2, r, :].astype(F32)
@@ -375,7 +378,7 @@
             po[m, pl.ds(k0, 2), :, cols] = r[ROWS:].reshape(2, HALF, 512)
             return 0
 
-        lax.fori_loop(0, NFS // 4, body, 0)
+        lax.fori_loop(0, NFS // 4, body, 0, unroll=2)
         pair_copy(l, m, k0).start()
         pair_copy(l, m, k0 + 1).start()
 
@@ -454,8 +457,32 @@
     peers = [right, left, partner] + [(fs_of(*d), tp) for d in ((0, 1), (0, 3), (1, 0), (3, 0))]
     for dev in peers:
         pl.semaphore_signal(barrier, inc=1, device_id=dev, device_id_type=MESH)
-    load_ffn(w1, g1, u1, d1, wl.at[0])
+    def fetch(k, *pairs):
+        for src, dst in pairs:
+            pltpu.make_async_copy(src, dst, fetched.at[k]).start()
+
+    def fetched_all(k, *refs):
+        for ref in refs:
+            pltpu.make_async_copy(ref, ref, fetched.at[k]).wait()
+
+    fetch(0, (tok_in, tok))
+    fetch(1, (s1_in, s1))
+    fetch(2, (g1_in, g1))
+    fetch(3, (u1_in, u1))
+    later = (
+        (s2_in, s2), (s3_in, s3), (g3_in, g3), (u3_in, u3), (ck_in, ck), (decay_in, decay),
+        (inputs_in, inputs), (cdw_in, cdw), (extra_in, extra),
+    )
+    for k, pair in enumerate(later):
+        fetch(4 + k, pair)
+    pltpu.make_async_copy(d1, w1.at[fs, pl.ds(0, HID)], wl.at[0]).start()
     load_mix(w2, wl.at[1])
+    pltpu.make_async_copy(d3, w3.at[fs, pl.ds(0, HID)], wl.at[2]).start()
+    fetched_all(2, g1)
+    fetched_all(3, u1)
+    load_ffn(w1, g1, u1)
+    fetched_all(0, tok)
+    fetched_all(1, s1)
     first_norm()
     pl.semaphore_wait(barrier, len(peers))
 
@@ -468,7 +495,9 @@
     ga, gc = gather_steps(0, 0), gather_steps(0, 1)
     ga[0]()
     gc[0]()
-    load_ffn(w3, g3, u3, d3, wl.at[2])
+    for k, pair in enumerate(later):
+        fetched_all(4 + k, pair[1])
+    load_ffn(w3, g3, u3)
     gate_map()
     gate_rates()
     rc[:, pl.ds(0, 8), :] = jnp.zeros((8, 8, CH), F32)
@@ -489,14 +518,13 @@
     ga[4]()
     gc[4]()
     ai[6]()
+    ad[0]()
     ai[7]()
-    ad[0]()
+    run(ad[1:4])
     ai[8]()
-    ad[1]()
-    ad[2]()
-    ffn_in(w1, 0, (ad[3], ad[4]))
-    ad[5]()
-    ffn_in(w1, 1, (ad[6], ad[7]))
+    ad[4]()
+    ffn_in(w1, 0, (ad[5], ad[6]))
+    ffn_in(w1, 1, (ad[7],))
     a2[0]()
     ad[8]()
 
@@ -534,7 +562,7 @@
     gates_half(1)
     gates(0, 8, 0, 8)
     run(a3[1:3])
-    lax.fori_loop(0, SEQ // T, scan_chunk, jnp.zeros((1, CH), F32))
+    lax.fori_loop(0, SEQ // T, scan_chunk, jnp.zeros((1, CH), F32), unroll=2)
 
     send_half(1, w2, CH, 0)
     a3[3]()
@@ -559,9 +587,12 @@
     a3[8]()
     ga[4]()
     ffn_in(w3, 0, (gc[1],))
-    send_half(2, w3, HPAD, 0)
     gc[2]()
+    project(2, w3, HPAD, 0, (2, 1))
+    post_first(2, 0)
     gc[3]()
+    project(2, w3, HPAD, 0, (3, 0))
+    post_second(2, 0)
     gc[4]()
     ffn_in(w3, 1, (lambda: post_ring(2, 0),))
     project(2, w3, HPAD, 1, (2, 1))
@@ -569,27 +600,46 @@
     project(2, w3, HPAD, 1, (3, 0))
     post_second(2, 1)
     finish(2, 0, res, 0.5, None, out)
+    top = pl.ds(0, HALF)
+    pltpu.make_async_copy(out.at[top], out_hbm.at[top], leave.at[0]).start()
     ai[9]()
     ad[9]()
     a2[9]()
     a3[9]()
     post_ring(2, 1)
     finish(2, 1, res, 0.5, None, out)
+    rest = pl.ds(HALF, HALF)
+    pltpu.make_async_copy(out.at[rest], out_hbm.at[rest], leave.at[1]).start()
+    for k, r in ((0, top), (1, rest)):
+        pltpu.make_async_copy(out.at[r], out_hbm.at[r], leave.at[k]).wait()
 
 
 def shards(
     tokens, s1, g1, u1, d1, s2, ri, og, ck, decay, inputs, cdw, extra, mo, s3, g3, u3, d3
 ):
-    vmem = pl.BlockSpec(memory_space=pltpu.VMEM)
-    hbm = pl.BlockSpec(memory_space=pl.ANY)
+    hbm = pl.BlockSpec(memory_space=pltpu.HBM)
     row = lambda v: v.reshape(1, -1)
     dma = pltpu.SemaphoreType.DMA
     return pl.pallas_call(
         layer_kernel,
         out_shape=jax.ShapeDtypeStruct((ROWS, D), BF16),
-        in_specs=[vmem] * 13 + [hbm] * 5,
-        out_specs=vmem,
+        in_specs=[hbm] * 18,
+        out_specs=hbm,
         scratch_shapes=[
+            pltpu.VMEM((ROWS, D), BF16),
+            pltpu.VMEM((ROWS, D), BF16),
+            pltpu.VMEM((1, D), F32),
+            pltpu.VMEM((1, D), F32),
+            pltpu.VMEM((1, D), F32),
+            pltpu.VMEM((HID, 128), BF16),
+            pltpu.VMEM((HID, 128), BF16),
+            pltpu.VMEM((HID, 128), BF16),
+            pltpu.VMEM((HID, 128), BF16),
+            pltpu.VMEM((4, CH), F32),
+            pltpu.VMEM((2, BLK, BLK), BF16),
+            pltpu.VMEM((2, BLK, BLK), BF16),
+            pltpu.VMEM((3, 128), F32),
+            pltpu.VMEM((8, 128), F32),
             pltpu.VMEM((NFS, FFN_ROWS, 128), BF16),
             pltpu.VMEM((NFS, MIX_ROWS, 128), BF16),
             pltpu.VMEM((NFS, FFN_ROWS, 128), BF16),
@@ -608,6 +658,8 @@
             pltpu.VMEM((CH, 2 * CH), BF16),
             pltpu.VMEM((3, 128), F32),
             pltpu.VMEM((8, 128, 128), F32),
+            dma((13,)),
+            dma((2,)),
             dma((3,)),
             dma((4,)),
             dma((2, 40)),
@@ -619,7 +671,7 @@
             dma((2, 2, 3)),
         ],
         compiler_params=pltpu.CompilerParams(
-            collective_id=0, has_side_effects=True, vmem_limit_bytes=60 * 1024 * 1024
+            collective_id=0, has_side_effects=True, vmem_limit_bytes=62 * 1024 * 1024
         ),
         name="layer",
     )(

time: 173 us -> 166 us (0.960)
  Pallas kernels: 171 us -> 164 us
    pallas_call x1, Pallas kernels: 171 us -> 164 us  [shards(): pl.pallas_call(layer_kernel, out_shape=jax.ShapeDtypeStruct((ROWS, D), BF...]
where the time goes in v4:
time: 166 us
  Pallas kernels  164 us (99%)
  local copies, waits for them, and re-layouts  1.88 us (1%)
    pallas_call x1, Pallas kernels, shards(): pl.pallas_call(layer_kernel, out_shape=jax.ShapeDtypeStruct((ROWS, D), BF...  164 us

profile of v4, /device:TPU:1, one launch (start us, length us, event | category | flops | bytes accessed | tf_op | source)
XLA Modules:
  0.0 165.6 jit_solution(6254836154480130761)
XLA Ops:
  0.0 163.7 %layer.1 = bf16[128,2048]{1,0:T(8,128)(2,1)} custom-call(bf16[128,2048]{1,0:T(8,128)(2,1)} %tok_in.1, f32[1,2048]{1,0:T(1,128)} %bitcast.13, f32[1,2048]{1,0:T(1,128)} %bitcast.14, f32[1,2048]{1,0:T(1,128)} %bitcast.15, bf16[688,128]{1,0:T(8,128)(2,1)} %bitcast.9, bf16[688,128]{1,0:T(8,128)(2,1)} %bitcast.10, bf16[688,128]{1,0:T(8,128)(2,1)} %bitcast.11, ...), custom_call_target="tpu_custom_call" | custom-call | tf_op jit(solution)/shard_map/layer/pallas_call | solution.py:623
  163.8 1.9 %copy.20 = bf16[128,2048]{1,0:T(8,128)(2,1)} copy(bf16[128,2048]{1,0:T(8,128)(2,1)} %layer.1) | data formatting | bytes 1048576

commit v5 on v4

--- a/solution.py
+++ b/solution.py
@@ -274,7 +274,9 @@
             r = jnp.dot(lhs, rhs, preferred_element_type=F32).astype(BF16)
             cols = pl.ds(pl.multiple_of(j * 128, 128), 128)
             rc[:, pl.ds(8 + HALF * m, HALF), cols] = r[:, :128].astype(F32).reshape(8, HALF, 128)
-            br[:, pl.ds(HALF * m, HALF), cols] = r[:, 128:].reshape(8, HALF, 128)
+            v = r[:, 128:].astype(F32)
+            v = 0.5 * v * (1.0 + jnp.tanh(0.7978845608028654 * (v + 0.044715 * v * v * v)))
+            br[:, pl.ds(HALF * m, HALF), cols] = v.reshape(8, HALF, 128)
             return 0
 
         lax.fori_loop(0, CH // 128, body, 0, unroll=True)
@@ -332,7 +334,7 @@
             gates(4 * i, 4, HALF * m, HALF)
             return 0
 
-        lax.fori_loop(0, 2, body, 0)
+        lax.fori_loop(0, 2, body, 0, unroll=True)
 
     T = 64
 
@@ -351,9 +353,7 @@
                 a = jnp.concatenate([a[:s], a[s:] * a[:-s]], axis=0)
             s *= 2
         state = b + a * carry
-        v = br[i // 2, r, :].astype(F32)
-        gelu = 0.5 * v * (1.0 + jnp.tanh(0.7978845608028654 * (v + 0.044715 * v * v * v)))
-        hid[i // 2, r, pl.ds(0, CH)] = (gelu * state).astype(BF16)
+        hid[i // 2, r, pl.ds(0, CH)] = (br[i // 2, r, :] * state).astype(BF16)
         return state[T - 1 : T, :]
 
     SLOT = {2: 0, 1: 1, 3: 2, 0: 3}
@@ -378,7 +378,7 @@
             po[m, pl.ds(k0, 2), :, cols] = r[ROWS:].reshape(2, HALF, 512)
             return 0
 
-        lax.fori_loop(0, NFS // 4, body, 0, unroll=2)
+        lax.fori_loop(0, NFS // 4, body, 0, unroll=True)
         pair_copy(l, m, k0).start()
         pair_copy(l, m, k0 + 1).start()
 
@@ -562,7 +562,7 @@
     gates_half(1)
     gates(0, 8, 0, 8)
     run(a3[1:3])
-    lax.fori_loop(0, SEQ // T, scan_chunk, jnp.zeros((1, CH), F32), unroll=2)
+    lax.fori_loop(0, SEQ // T, scan_chunk, jnp.zeros((1, CH), F32), unroll=4)
 
     send_half(1, w2, CH, 0)
     a3[3]()
@@ -589,15 +589,15 @@
     ffn_in(w3, 0, (gc[1],))
     gc[2]()
     project(2, w3, HPAD, 0, (2, 1))
+    project(2, w3, HPAD, 0, (3, 0))
     post_first(2, 0)
     gc[3]()
-    project(2, w3, HPAD, 0, (3, 0))
     post_second(2, 0)
     gc[4]()
-    ffn_in(w3, 1, (lambda: post_ring(2, 0),))
+    ffn_in(w3, 1, (lambda: None, lambda: post_ring(2, 0)))
     project(2, w3, HPAD, 1, (2, 1))
+    project(2, w3, HPAD, 1, (3, 0))
     post_first(2, 1)
-    project(2, w3, HPAD, 1, (3, 0))
     post_second(2, 1)
     finish(2, 0, res, 0.5, None, out)
     top = pl.ds(0, HALF)
@@ -652,7 +652,7 @@
             pltpu.VMEM((2, 2, 3, QUART, D), BF16),
             pltpu.VMEM((ROWS, D), BF16),
             pltpu.VMEM((8, ROWS + 8, CH), F32),
-            pltpu.VMEM((8, ROWS, CH), BF16),
+            pltpu.VMEM((8, ROWS, CH), F32),
             pltpu.VMEM((8, ROWS, CH), F32),
             pltpu.VMEM((8, ROWS, CH), F32),
             pltpu.VMEM((CH, 2 * CH), BF16),

time: 166 us -> 165 us (level)
  Pallas kernels: 164 us -> 162 us
where the time goes in v5:
time: 165 us; the launch traced here: 164 us
  Pallas kernels  162 us (98%)
  local copies, waits for them, and re-layouts  1.88 us (1%)
    pallas_call x1, Pallas kernels, shards(): pl.pallas_call(layer_kernel, out_shape=jax.ShapeDtypeStruct((ROWS, D), BF...  162 us

profile of v5, /device:TPU:1, one launch (start us, length us, event | category | flops | bytes accessed | tf_op | source)
XLA Modules:
  0.0 164.4 jit_solution(1031523419665840429)
XLA Ops:
  0.0 162.5 %layer.1 = bf16[128,2048]{1,0:T(8,128)(2,1)} custom-call(bf16[128,2048]{1,0:T(8,128)(2,1)} %tok_in.1, f32[1,2048]{1,0:T(1,128)} %bitcast.13, f32[1,2048]{1,0:T(1,128)} %bitcast.14, f32[1,2048]{1,0:T(1,128)} %bitcast.15, bf16[688,128]{1,0:T(8,128)(2,1)} %bitcast.9, bf16[688,128]{1,0:T(8,128)(2,1)} %bitcast.10, bf16[688,128]{1,0:T(8,128)(2,1)} %bitcast.11, ...), custom_call_target="tpu_custom_call" | custom-call | tf_op jit(solution)/shard_map/layer/pallas_call | solution.py:623
  162.5 1.9 %copy.20 = bf16[128,2048]{1,0:T(8,128)(2,1)} copy(bf16[128,2048]{1,0:T(8,128)(2,1)} %layer.1) | data formatting | bytes 1048576
